TPU v7x, 256 devices: a whole 4x4x8 slice. The times are simulated.
256 devices in a mesh: sp: 64 (over z, x, core), tp: 4 (over y).
Axes of the slice: x: 4, y: 4, z: 8, core: 2. Of those that a mesh axis runs over, the one named last changes fastest.
Arguments:
- tokens: bfloat16 [16384, 2048], P(('sp', 'tp')), may hold values from -6 to 6
- input_gain: float32 [2048], replicated, may hold values from 0.1 to 1.9
- memory_query: bfloat16 [2048, 512], P(None, 'tp'), may hold values from -0.125 to 0.125
- memory_key: bfloat16 [2048, 512], P(None, 'tp'), may hold values from -0.125 to 0.125
- memory_value: bfloat16 [2048, 512], P(None, 'tp'), may hold values from -0.125 to 0.125
- memory_outgate: bfloat16 [2048, 512], P(None, 'tp'), may hold values from -0.125 to 0.125
- memory_gates: bfloat16 [2048, 4, 8], replicated, may hold values from -0.0625 to 0.0625
- gate_offset: float32 [4, 16384, 8], P(None, 'sp', 'tp'), may hold values from -1 to 150
- memory_norm_gain: float32 [512], replicated, may hold values from 0.1 to 1.9
- query_down: bfloat16 [2048, 384], replicated, may hold values from -0.125 to 0.125
- query_down_gain: float32 [384], replicated, may hold values from 0.1 to 1.9
- latent_down: bfloat16 [2048, 256], replicated, may hold values from -0.125 to 0.125
- latent_gain: float32 [256], replicated, may hold values from 0.1 to 1.9
- rotary_down: bfloat16 [2048, 32], replicated, may hold values from -0.125 to 0.125
- query_up: bfloat16 [384, 8, 96], replicated, may hold values from -0.3125 to 0.3125
- latent_up: bfloat16 [256, 8, 128], replicated, may hold values from -0.375 to 0.375
- query_gain: float32 [96], replicated, may hold values from 1.2 to 8
- key_gain: float32 [96], replicated, may hold values from 1.2 to 8
- memory_output: bfloat16 [512, 2048], replicated, may hold values from -0.25 to 0.25
- attention_output: bfloat16 [512, 2048], replicated, may hold values from -0.75 to 0.75
Outputs:
- mixed: bfloat16 [16384, 2048], P(('sp', 'tp'))
All inputs are finite; a program needn't handle non-finite values.
Results may differ from a plain program's by a relative error of at most 0.019.
The roundings to bfloat16 on the way count: a program that leaves them out, or rounds other values in their place, can miss the bound.
Values may be sent and summed in bfloat16 or wider, within the bound.
A program may use at most 128 MiB of HBM per device.

v0:
```python
import jax
import jax.numpy as jnp
from jax import lax
from jax.sharding import Mesh
from jax.sharding import PartitionSpec as P

MEMORY_HEADS = 8
ML_DH = 64
ML_BLOCK = 128
MLA_HEADS = 8
NOPE = 64
ROPE = 32
VDIM = 64
SP = ("sp_0", "sp_1", "sp_2")
SP_TP = ("sp_0", "sp_1", "sp_2", "tp")


EPSILON = 1e-06
ROPE_BASE = 10000.0
FLOOR_LOG = -1e30
SCORE_LIMIT = 4096


def copy_for_each(value, axis):
    length = lax.axis_size(axis)
    return lax.all_to_all(
        jnp.broadcast_to(value[None], (length, *value.shape)), axis, 0, 0, tiled=True
    )


def in_order(parts, dim):
    parts = jnp.moveaxis(parts, 0, dim)
    shape = parts.shape
    return parts.reshape(*shape[:dim], shape[dim] * shape[dim + 1], *shape[dim + 2 :])


def gathered_copies(value, axis, dim):
    parts = copy_for_each(value, axis)
    return in_order(parts, dim)


def neutral_like(value, identity):
    return jax.tree.map(
        lambda part, zero: jnp.zeros_like(part) + jnp.asarray(zero, part.dtype), value, identity
    )


def collected_together(value, axis):
    leaves = jax.tree.leaves(value)
    sequence = sorted(range(len(leaves)), key=lambda k: -leaves[k].size)
    width = (1, *leaves[sequence[0]].shape)[-1]
    lines = [
        jnp.pad(leaves[k].reshape(-1), (0, -leaves[k].size % width)).reshape(-1, width)
        for k in sequence
    ]
    both, at, found = (lax.all_gather(jnp.concatenate(lines), axis), 0, {})
    for k, line in zip(sequence, lines):
        section = both[:, at : at + len(line)].reshape(len(both), -1)
        found[k] = section[:, : leaves[k].size].reshape(-1, *leaves[k].shape)
        at += len(line)
    numbers = iter(range(len(leaves)))
    return jax.tree.map(lambda _: found[next(numbers)], value)


def prefix_by_axis(value, axes, combine, identity, reverse):
    before = start = neutral_like(value, identity)
    subtotal = value
    for axis in reversed(axes):
        length, mine = (lax.axis_size(axis), lax.axis_index(axis))
        pieces = collected_together(subtotal, axis)
        inside, subtotal = (start, start)
        for k in reversed(range(length)) if reverse else range(length):
            passed = k > mine if reverse else k < mine
            subtotal = combine(subtotal, jax.tree.map(lambda part: part[k], pieces))
            inside = jax.tree.map(lambda new, old: jnp.where(passed, new, old), subtotal, inside)
        before = combine(inside, before)
    return before


def side_by_side(arrays, axis, dim, along):
    both = jnp.concatenate(arrays, axis=along)
    out, at, finished = (lax.all_gather(both, axis, axis=dim, tiled=True), 0, [])
    for a in arrays:
        finished.append(lax.slice_in_dim(out, at, at + a.shape[along], axis=along))
        at += a.shape[along]
    return tuple(finished)


def rounded(vectors):
    return lax.optimization_barrier(vectors.astype(jnp.bfloat16))


def rms_scale(vectors, scaling):
    mean_square = jnp.mean(vectors * vectors, axis=-1, keepdims=True)
    return vectors * lax.rsqrt(mean_square + EPSILON) * scaling


def rotate_half(vectors, positions):
    half_width = vectors.shape[-1] // 2
    frequency = ROPE_BASE ** (-jnp.arange(half_width, dtype=jnp.float32) / half_width)
    angles = positions.astype(jnp.float32)[:, None] * frequency[None, :]
    shaped = (positions.shape[0],) + (1,) * (vectors.ndim - 2) + (half_width,)
    cosine = jnp.cos(angles).reshape(shaped)
    sine_part = jnp.sin(angles).reshape(shaped)
    first_half = vectors[..., :half_width]
    second_half = vectors[..., half_width:]
    return jnp.concatenate(
        [
            first_half * cosine - second_half * sine_part,
            first_half * sine_part + second_half * cosine,
        ],
        axis=-1,
    )


def memory_local(queries, key_rows, value_rows, in_gate, log_forget):
    length = queries.shape[0]
    head_count = queries.shape[1]
    head_width = queries.shape[2]
    lower_mask = jnp.tril(jnp.ones((ML_BLOCK, ML_BLOCK), dtype=bool))
    memory = jnp.zeros((head_count, head_width, head_width), jnp.float32)
    normal = jnp.zeros((head_count, head_width), jnp.float32)
    stabilizer = jnp.full((head_count,), FLOOR_LOG, jnp.float32)
    numerators = []
    denominators = []
    toplevels = []
    for offset in range(0, length, ML_BLOCK):
        query_block = queries[offset : offset + ML_BLOCK]
        key_block = key_rows[offset : offset + ML_BLOCK]
        value_block = value_rows[offset : offset + ML_BLOCK]
        gate_block = in_gate[offset : offset + ML_BLOCK]
        cumulated = jnp.cumsum(log_forget[offset : offset + ML_BLOCK], axis=0)
        decays = cumulated[:, None, :] - cumulated[None, :, :] + gate_block[None, :, :]
        decays = jnp.where(lower_mask[:, :, None], decays, -jnp.inf)
        carried_log = cumulated + stabilizer[None, :]
        topmost = jnp.maximum(carried_log, jnp.max(decays, axis=1))
        scores = jnp.einsum(
            "thd,shd->tsh", query_block, key_block, preferred_element_type=jnp.float32
        )
        weights = scores * jnp.exp(decays - topmost[:, None, :])
        numerator = jnp.einsum(
            "tsh,shd->thd",
            weights.astype(jnp.bfloat16),
            value_block,
            preferred_element_type=jnp.float32,
        )
        denominator = jnp.sum(weights, axis=1)
        carried = jnp.exp(carried_log - topmost)
        query_float = query_block.astype(jnp.float32)
        numerator = numerator + carried[:, :, None] * jnp.einsum(
            "hvk,thk->thv", memory, query_float, precision=lax.Precision.HIGHEST
        )
        denominator = denominator + carried * jnp.einsum(
            "hk,thk->th", normal, query_float, precision=lax.Precision.HIGHEST
        )
        numerators.append(numerator)
        denominators.append(denominator)
        toplevels.append(topmost)
        key_float = key_block.astype(jnp.float32)
        last_total = cumulated[-1]
        growth = last_total[None, :] - cumulated + gate_block
        next_level = jnp.maximum(last_total + stabilizer, jnp.max(growth, axis=0))
        inflow = jnp.exp(growth - next_level[None, :])
        shrink = jnp.exp(last_total + stabilizer - next_level)
        weighted = inflow[:, :, None] * value_block.astype(jnp.float32)
        memory = shrink[:, None, None] * memory + jnp.einsum(
            "shv,shk->hvk", weighted, key_float, precision=lax.Precision.HIGHEST
        )
        normal = shrink[:, None] * normal + jnp.einsum(
            "sh,shk->hk", inflow, key_float, precision=lax.Precision.HIGHEST
        )
        stabilizer = next_level
    total_log = jnp.sum(log_forget, axis=0)
    partials = (
        jnp.concatenate(numerators, axis=0),
        jnp.concatenate(denominators, axis=0),
        jnp.concatenate(toplevels, axis=0),
    )
    return (partials, (memory, normal, stabilizer, total_log))


def chain(earlier, later):
    memory_early, normal_early, level_early, total_early = earlier
    memory_late, normal_late, level_late, total_late = later
    joined = jnp.maximum(total_late + level_early, level_late)
    scale_early = jnp.exp(total_late + level_early - joined)
    scale_late = jnp.exp(level_late - joined)
    return (
        scale_early[:, None, None] * memory_early + scale_late[:, None, None] * memory_late,
        scale_early[:, None] * normal_early + scale_late[:, None] * normal_late,
        joined,
        total_early + total_late,
    )


def memory_finish(partials, queries, log_forget, incoming):
    numerator, denominator, topmost = partials
    memory = incoming[0]
    normal = incoming[1]
    level = incoming[2]
    carried_log = jnp.cumsum(log_forget, axis=0) + level[None, :]
    joined = jnp.maximum(topmost, carried_log)
    own_scale = jnp.exp(topmost - joined)
    carried = jnp.exp(carried_log - joined)
    query_float = queries.astype(jnp.float32)
    numerator = numerator * own_scale[:, :, None] + carried[:, :, None] * jnp.einsum(
        "hvk,thk->thv", memory, query_float, precision=lax.Precision.HIGHEST
    )
    denominator = denominator * own_scale + carried * jnp.einsum(
        "hk,thk->th", normal, query_float, precision=lax.Precision.HIGHEST
    )
    return numerator / jnp.maximum(jnp.abs(denominator), jnp.exp(-joined))[:, :, None]


def attention_fold(queries_att, key_weight, plain_gain):
    head_count = queries_att.shape[1]
    query_plain = queries_att[..., :NOPE]
    query_turned = queries_att[..., NOPE:]
    row_limit = max(SCORE_LIMIT // head_count, 128)

    def absorb(state_carry, pieces, start_row):
        latent, rotary = pieces
        piece_rows = latent.shape[0]
        block_rows = piece_rows
        while block_rows > row_limit and block_rows % 2 == 0:
            block_rows = block_rows // 2

        def one_block(index, running):
            topmost, totals, accumulated = running
            latent_block = lax.dynamic_slice_in_dim(latent, index * block_rows, block_rows, 0)
            rotary_block = lax.dynamic_slice_in_dim(rotary, index * block_rows, block_rows, 0)
            expanded = jnp.dot(latent_block, key_weight, preferred_element_type=jnp.float32)
            expanded = expanded.reshape(block_rows, head_count, NOPE + VDIM)
            key_plain = rms_scale(expanded[..., :NOPE], plain_gain).astype(jnp.bfloat16)
            value_block = expanded[..., NOPE:].astype(jnp.bfloat16)
            scores = jnp.einsum(
                "thd,shd->hts", query_plain, key_plain, preferred_element_type=jnp.float32
            ) + jnp.einsum(
                "thr,sr->hts", query_turned, rotary_block, preferred_element_type=jnp.float32
            )
            new_top = jnp.maximum(topmost, jnp.max(scores, axis=-1))
            correction = jnp.exp(topmost - new_top)
            lifted = jnp.exp(scores - new_top[..., None])
            totals = totals * correction + jnp.sum(lifted, axis=-1)
            accumulated = accumulated * correction[..., None] + jnp.einsum(
                "hts,shd->htd",
                lifted.astype(jnp.bfloat16),
                value_block,
                preferred_element_type=jnp.float32,
            )
            return (new_top, totals, accumulated)

        return lax.fori_loop(0, piece_rows // block_rows, one_block, state_carry)

    return absorb


def make_queries(query_latent, up_weight, head_count, positions, query_gain):
    length = query_latent.shape[0]
    query_full = jnp.dot(
        query_latent,
        up_weight.reshape(up_weight.shape[0], head_count * (NOPE + ROPE)),
        preferred_element_type=jnp.float32,
    ).reshape(length, head_count, NOPE + ROPE)
    query_plain = rms_scale(query_full[..., :NOPE], query_gain[:NOPE])
    query_turned = rotate_half(rms_scale(query_full[..., NOPE:], query_gain[NOPE:]), positions)
    return (jnp.concatenate([query_plain, query_turned], axis=-1) * (NOPE + ROPE) ** (-0.5)).astype(
        jnp.bfloat16
    )


def empty_state(head_count, length):
    return (
        jnp.full((head_count, length), FLOOR_LOG, jnp.float32),
        jnp.zeros((head_count, length), jnp.float32),
        jnp.zeros((head_count, length, VDIM), jnp.float32),
    )


def body(
    tokens,
    input_gain,
    memory_query,
    memory_key,
    memory_value,
    memory_outgate,
    memory_gates,
    gate_offset,
    memory_norm_gain,
    query_down,
    query_down_gain,
    latent_down,
    latent_gain,
    rotary_down,
    query_up,
    latent_up,
    query_gain,
    key_gain,
    memory_output,
    attention_output,
):
    groups = lax.axis_size("tp")
    member = lax.axis_index("tp")
    segment = lax.axis_index(SP)
    local_rows = tokens.shape[0]
    length = local_rows * groups
    normed_local = rms_scale(tokens.astype(jnp.float32), input_gain).astype(jnp.bfloat16)
    normed = gathered_copies(normed_local, "tp", 0)
    positions = segment * length + jnp.arange(length, dtype=jnp.int32)

    def project(weight_matrix):
        return jnp.dot(normed, weight_matrix, preferred_element_type=jnp.float32)

    mem_heads = MEMORY_HEADS // groups
    mem_shape = (length, mem_heads, ML_DH)
    queries_mem = project(memory_query).astype(jnp.bfloat16).reshape(mem_shape)
    keys_mem = (project(memory_key) * ML_DH ** (-0.5)).astype(jnp.bfloat16).reshape(mem_shape)
    values_mem = project(memory_value).astype(jnp.bfloat16).reshape(mem_shape)
    outgate = rounded(project(memory_outgate)).astype(jnp.float32)
    gate_columns = lax.dynamic_slice_in_dim(memory_gates, member * mem_heads, mem_heads, 2)
    gate_data = rounded(project(gate_columns.reshape(gate_columns.shape[0], 4 * mem_heads)))
    gate_pre = gate_data.astype(jnp.float32).reshape(length, 4, mem_heads) + jnp.transpose(
        gate_offset, (1, 0, 2)
    )
    forward_forget = jax.nn.log_sigmoid(gate_pre[:, 1])
    backward_forget = jnp.flip(jax.nn.log_sigmoid(gate_pre[:, 3]), 0)
    backward_queries = jnp.flip(queries_mem, 0)
    forward_parts, forward_state = memory_local(
        queries_mem, keys_mem, values_mem, gate_pre[:, 0], forward_forget
    )
    backward_parts, backward_state = memory_local(
        backward_queries,
        jnp.flip(keys_mem, 0),
        jnp.flip(values_mem, 0),
        jnp.flip(gate_pre[:, 2], 0),
        backward_forget,
    )
    identity = (
        jnp.zeros_like(forward_state[0]),
        jnp.zeros_like(forward_state[1]),
        jnp.full_like(forward_state[2], FLOOR_LOG),
        jnp.zeros_like(forward_state[3]),
    )
    forward_in = prefix_by_axis(
        (forward_state[0], forward_state[1], forward_state[2], forward_state[3]),
        SP,
        chain,
        identity,
        False,
    )
    backward_in = prefix_by_axis(
        (backward_state[0], backward_state[1], backward_state[2], backward_state[3]),
        SP,
        chain,
        identity,
        True,
    )
    forward_out = memory_finish(forward_parts, queries_mem, forward_forget, forward_in)
    backward_out = jnp.flip(
        memory_finish(backward_parts, backward_queries, backward_forget, backward_in), 0
    )
    norm_slice = lax.dynamic_slice_in_dim(
        memory_norm_gain, member * mem_heads * ML_DH, mem_heads * ML_DH, 0
    )
    combined = rms_scale(forward_out + backward_out, norm_slice.reshape(mem_heads, ML_DH))
    memory_rows = (combined.reshape(length, mem_heads * ML_DH) * jax.nn.sigmoid(outgate)).astype(
        jnp.bfloat16
    )
    att_heads = MLA_HEADS // groups
    query_latent = rms_scale(project(query_down), query_down_gain).astype(jnp.bfloat16)
    up_slice = lax.dynamic_slice_in_dim(query_up, member * att_heads, att_heads, 1)
    queries_att = make_queries(query_latent, up_slice, att_heads, positions, query_gain)
    key_slice = lax.dynamic_slice_in_dim(latent_up, member * att_heads, att_heads, 1)
    key_weight = key_slice.reshape(key_slice.shape[0], att_heads * (NOPE + VDIM))
    absorb = attention_fold(queries_att, key_weight, key_gain[:NOPE])
    latent = rms_scale(
        jnp.dot(normed, latent_down, preferred_element_type=jnp.float32), latent_gain
    ).astype(jnp.bfloat16)
    rotary = rotate_half(
        rms_scale(
            jnp.dot(normed, rotary_down, preferred_element_type=jnp.float32), key_gain[NOPE:]
        ),
        positions,
    ).astype(jnp.bfloat16)
    latent, rotary = (latent, rotary)
    folded = absorb(
        empty_state(att_heads, length), side_by_side((latent, rotary), SP, 0, 1), jnp.int32(0)
    )
    attention_rows = jnp.transpose(
        (folded[2] / folded[1][:, :, None]).astype(jnp.bfloat16), (1, 0, 2)
    )
    attention_rows = attention_rows.reshape(length, att_heads * VDIM)
    mem_part, att_part = (
        lax.all_to_all(memory_rows, "tp", split_axis=0, concat_axis=1, tiled=True),
        lax.all_to_all(attention_rows, "tp", split_axis=0, concat_axis=1, tiled=True),
    )
    mixed = jnp.dot(mem_part, memory_output, preferred_element_type=jnp.float32) + jnp.dot(
        att_part, attention_output, preferred_element_type=jnp.float32
    )
    return mixed.astype(jnp.bfloat16)


def solution(mesh):
    split = Mesh(mesh.devices.reshape(8, 4, 2, mesh.shape["tp"]), ("sp_0", "sp_1", "sp_2", "tp"))
    in_specs = (
        P(SP_TP, None),
        P(),
        P(None, "tp"),
        P(None, "tp"),
        P(None, "tp"),
        P(None, "tp"),
        P(),
        P(None, SP, "tp"),
        P(),
        P(),
        P(),
        P(),
        P(),
        P(),
        P(),
        P(),
        P(),
        P(),
        P(),
        P(),
    )
    out_specs = P(SP_TP, None)
    return jax.shard_map(body, mesh=split, in_specs=in_specs, out_specs=out_specs, check_vma=False)
```

profile of v0, /device:TPU:2, one launch (start us, length us, event | category | flops | bytes accessed | tf_op | source)
XLA Modules:
  0.0 361.3 jit_solution(17531555069814887451)
XLA Ops:
  6.5 1.2 fusion.40
  7.8 1.1 fusion.42
  8.9 1.1 broadcast_in_dim.49
  10.0 4.5 %all-to-all-start = ((bf16[4,64,2048]{2,1,0:T(8,128)(2,1)}), bf16[4,64,2048]{2,1,0:T(8,128)(2,1)S(1)}, u32[]{:S(2)}, u32[]{:S(2)}) async-start(bf16[4,64,2048]{2,1,0:T(8,128)(2,1)} %broadcast_in_dim.49), calls=%async_computation | async-start | bytes 2097152 | tf_op jit(solution)/shard_map/all_to_all | solution.py:26
  18.7 1.2 constant_dynamic-slice_fusion
  20.1 1.0 copy.285
  21.7 7.8 %all-to-all-done = bf16[4,64,2048]{2,1,0:T(8,128)(2,1)S(1)} async-done(((bf16[4,64,2048]{2,1,0:T(8,128)(2,1)}), bf16[4,64,2048]{2,1,0:T(8,128)(2,1)S(1)}, u32[]{:S(2)}, u32[]{:S(2)}) %all-to-all-start) | async-done | bytes 1048608 | tf_op jit(solution)/shard_map/all_to_all | solution.py:26
  29.6 2.2 multiply_reduce_fusion.1
  31.8 1.2 fusion.44
  33.1 1.3 multiply_reduce_fusion.12
  36.6 1.0 copy.286
  37.6 1.3 bitcast_add_fusion.1
  39.8 1.4 fusion.198
  41.1 1.5 rev.15
  42.6 1.6 fusion.462
  44.3 1.6 reduce_window_sum.54
  45.9 1.3 slice_bitcast_fusion.7
  47.2 1.4 copy.287
  48.6 1.6 reduce_window_sum.55
  50.2 1.2 slice_bitcast_fusion.6
  51.4 1.5 copy.294
  52.9 1.5 slice.835
  54.4 1.6 reduce_window_sum.59
  56.0 1.3 slice_bitcast_fusion.4
  57.2 1.5 copy.356
  58.7 1.5 slice.827
  60.2 1.6 reduce_window_sum.58
  61.8 1.3 slice_bitcast_fusion.5
  63.1 1.5 copy.349
  64.6 1.5 convolution_convert_fusion.1
  68.7 1.4 copy.434
  70.1 1.5 rev.16
  71.6 2.1 convolution_convert_fusion
  73.7 1.5 fusion.31
  75.8 1.5 slice.832
  78.0 1.5 convolution_convert_fusion.2
  80.2 1.5 slice.831
  82.3 1.8 multiply_reduce_fusion.2
  110.9 1.9 all-gather.6
  124.6 1.9 all-gather.9
  137.6 13.1 %all-gather.7 = f32[4,132,64]{1,2,0:T(8,128)S(1)} all-gather(f32[1,132,64]{1,2,0:T(8,128)S(1)} %maximum_bitcast_fusion.1), channel_id=3, replica_groups=mesh['sp_0'=8,'sp_1'=4,'sp_2'=2,'tp'=4] {'sp_1'}, dimensions={0}, use_global_device_ids=true | all-gather | bytes 168960 | tf_op jit(solution)/shard_map/all_gather | solution.py:56
  154.1 13.5 %all-gather.10 = f32[4,132,64]{1,2,0:T(8,128)S(1)} all-gather(f32[1,132,64]{1,2,0:T(8,128)S(1)} %maximum_bitcast_fusion.4), channel_id=6, replica_groups=mesh['sp_0'=8,'sp_1'=4,'sp_2'=2,'tp'=4] {'sp_1'}, dimensions={0}, use_global_device_ids=true | all-gather | bytes 168960 | tf_op jit(solution)/shard_map/all_gather | solution.py:56
  182.8 28.5 %all-gather.8 = f32[8,132,64]{1,2,0:T(8,128)S(1)} all-gather(f32[1,132,64]{1,2,0:T(8,128)S(1)} %maximum_bitcast_fusion.2), channel_id=4, replica_groups=mesh['sp_0'=8,'sp_1'=4,'sp_2'=2,'tp'=4] {'sp_0'}, dimensions={0}, use_global_device_ids=true | all-gather | bytes 304128 | tf_op jit(solution)/shard_map/all_gather | solution.py:56
  217.3 1.1 copy.496
  226.5 25.2 %all-gather.11 = f32[8,132,64]{1,2,0:T(8,128)S(1)} all-gather(f32[1,132,64]{1,2,0:T(8,128)S(1)} %maximum_bitcast_fusion.5), channel_id=7, replica_groups=mesh['sp_0'=8,'sp_1'=4,'sp_2'=2,'tp'=4] {'sp_0'}, dimensions={0}, use_global_device_ids=true | all-gather | bytes 304128 | tf_op jit(solution)/shard_map/all_gather | solution.py:56
  264.0 1.0 fusion.467
  267.3 1.1 fusion.375
  275.8 1.7 fusion.26
  287.5 1.6 multiply_reduce_fusion.4
  290.0 3.9 %all-to-all-start.1 = ((bf16[4,64,128]{2,1,0:T(8,128)(2,1)}), bf16[4,64,128]{2,1,0:T(8,128)(2,1)}, u32[]{:S(2)}, u32[]{:S(2)}) async-start(bf16[4,64,128]{2,1,0:T(8,128)(2,1)} %bitcast.230), calls=%async_computation.1 | async-start | bytes 131072 | tf_op jit(solution)/shard_map/all_to_all | solution.py:394
  294.0 7.6 %slice.1015 = bf16[16384,256]{0,1:T(8,128)(2,1)} slice(bf16[16384,288]{0,1:T(8,128)(2,1)} %all-gather.14.cloned.1.call-done), slice={[0:16384], [0:256]} | slice | bytes 16777216 | tf_op jit(solution)/shard_map/slice | solution.py:84
  301.6 38.9 %while.18 = (s32[]{:T(128)}, f32[2,256]{1,0:T(2,128)S(1)}, f32[2,256]{1,0:T(2,128)S(1)}, f32[2,256,64]{1,2,0:T(8,128)S(1)}, bf16[16384,256]{0,1:T(8,128)(2,1)}, ...) while((s32[]{:T(128)}, f32[2,256]{1,0:T(2,128)S(1)}, ...), condition=%wide.region_33.34_spmd.clone, body=%wide.region_29.33_spmd.clone.sunk | while | flops 611686912 | bytes 27460300 | solution.py:253
  301.6 1.7 fusion.550
  306.5 1.7 fusion.550
  311.4 1.7 fusion.550
  316.2 1.7 fusion.550
  321.1 1.7 fusion.550
  325.9 1.7 fusion.550
  330.8 1.7 fusion.550
  335.6 1.7 fusion.550
  341.4 4.7 %all-to-all-start.2 = ((bf16[4,64,128]{2,1,0:T(8,128)(2,1)}), bf16[4,64,128]{2,1,0:T(8,128)(2,1)S(1)}, u32[]{:S(2)}, u32[]{:S(2)}) async-start(bf16[4,64,128]{2,1,0:T(8,128)(2,1)} %copy.492), calls=%async_computation.2 | async-start | bytes 131072 | tf_op jit(solution)/shard_map/all_to_all | solution.py:395
  346.1 1.3 fusion.60
  347.4 4.3 %all-to-all-done.2 = bf16[4,64,128]{2,1,0:T(8,128)(2,1)S(1)} async-done(((bf16[4,64,128]{2,1,0:T(8,128)(2,1)}), bf16[4,64,128]{2,1,0:T(8,128)(2,1)S(1)}, u32[]{:S(2)}, u32[]{:S(2)}) %all-to-all-start.2) | async-done | bytes 65568 | tf_op jit(solution)/shard_map/all_to_all | solution.py:395
  351.7 2.8 fusion.19
  (715 shorter events, 152.1 us)
Async XLA Ops:
  6.5 339.5 %copy-start = (bf16[512,2048]{1,0:T(8,128)(2,1)S(1)}, bf16[512,2048]{1,0:T(8,128)(2,1)}, u32[]{:S(2)}) copy-start(bf16[512,2048]{1,0:T(8,128)(2,1)} %param.40) | copy-start | bytes 6291460
  10.0 19.6 %all-to-all-start = ((bf16[4,64,2048]{2,1,0:T(8,128)(2,1)}), bf16[4,64,2048]{2,1,0:T(8,128)(2,1)S(1)}, u32[]{:S(2)}, u32[]{:S(2)}) async-start(bf16[4,64,2048]{2,1,0:T(8,128)(2,1)} %broadcast_in_dim.49), calls=%async_computation | async-start | bytes 2097152 | tf_op jit(solution)/shard_map/all_to_all | solution.py:26
  14.5 279.4 %all-gather.14.cloned.1.call-start = ((), (), s32[]{:S(2)}) async-start(), calls=%async_computation.3 | async-start | bytes 9584640 | tf_op jit(solution)/shard_map/all_gather | solution.py:82
  35.5 44.0 %copy-start.2 = (bf16[256,2,96]{0,2,1:T(8,128)(2,1)}, bf16[256,2,96]{0,2,1:T(8,128)(2,1)S(1)}, u32[]{:S(2)}) copy-start(bf16[256,2,96]{0,2,1:T(8,128)(2,1)S(1)} %fusion.46) | copy-start | bytes 294916
  80.2 12.6 %copy-start.3 = (f32[128,2]{1,0:T(8,128)S(1)}, f32[128,2]{1,0:T(8,128)}, u32[]{:S(2)}) copy-start(f32[128,2]{1,0:T(8,128)} %reduce_window_sum.59) | copy-start | bytes 3076
  82.3 12.1 %copy-start.4 = (f32[128,2]{1,0:T(8,128)S(1)}, f32[128,2]{1,0:T(8,128)}, u32[]{:S(2)}) copy-start(f32[128,2]{1,0:T(8,128)} %reduce_window_sum.55) | copy-start | bytes 3076
  84.2 12.3 %copy-start.6 = (f32[256,2]{1,0:T(8,128)S(1)}, f32[256,2]{1,0:T(8,128)}, u32[]{:S(2)}) copy-start(f32[256,2]{1,0:T(8,128)} %rev.15) | copy-start | bytes 6148
  84.2 14.7 %copy-start.7 = (f32[128,2]{1,0:T(8,128)S(1)}, f32[128,2]{1,0:T(8,128)}, u32[]{:S(2)}) copy-start(f32[128,2]{1,0:T(8,128)} %reduce_window_sum.58) | copy-start | bytes 3076
  84.2 14.7 %copy-start.136 = (f32[2]{0:T(128)S(1)}, f32[2]{0:T(128)}, u32[]{:S(2)}) copy-start(f32[2]{0:T(128)} %slice_bitcast_fusion.5) | copy-start | bytes 28
  84.2 15.3 %copy-start.119 = (f32[2]{0:T(128)S(1)}, f32[2]{0:T(128)}, u32[]{:S(2)}) copy-start(f32[2]{0:T(128)} %slice_bitcast_fusion.4) | copy-start | bytes 28
  84.2 16.5 %copy-start.32 = (bf16[128,2,64]{0,2,1:T(8,128)(2,1)S(1)}, bf16[128,2,64]{0,2,1:T(8,128)(2,1)}, u32[]{:S(2)}) copy-start(bf16[128,2,64]{0,2,1:T(8,128)(2,1)} %slice.832) | copy-start | bytes 98308
  84.2 17.4 %copy-start.51 = (pred[128,128]{0,1:T(8,128)(4,1)S(1)}, pred[128,128]{0,1:T(8,128)(4,1)}, u32[]{:S(2)}) copy-start(pred[128,128]{0,1:T(8,128)(4,1)} %iota_compare_fusion) | copy-start | bytes 49156
  84.2 17.4 %copy-start.65 = (f32[128,2]{0,1:T(2,128)S(1)}, f32[128,2]{0,1:T(2,128)}, u32[]{:S(2)}) copy-start(f32[128,2]{0,1:T(2,128)} %copy.294) | copy-start | bytes 3076
  84.2 17.4 %copy-start.66 = (f32[128,2]{0,1:T(2,128)S(1)}, f32[128,2]{0,1:T(2,128)}, u32[]{:S(2)}) copy-start(f32[128,2]{0,1:T(2,128)} %copy.287) | copy-start | bytes 3076
  84.2 17.4 %copy-start.67 = (f32[128,2]{0,1:T(2,128)S(1)}, f32[128,2]{0,1:T(2,128)}, u32[]{:S(2)}) copy-start(f32[128,2]{0,1:T(2,128)} %copy.356) | copy-start | bytes 3076
  84.2 17.4 %copy-start.68 = (f32[128,2]{0,1:T(2,128)S(1)}, f32[128,2]{0,1:T(2,128)}, u32[]{:S(2)}) copy-start(f32[128,2]{0,1:T(2,128)} %copy.349) | copy-start | bytes 3076
  84.3 18.5 %copy-start.37 = (f32[2,1,128]{0,2,1:T(8,128)S(1)}, f32[2,1,128]{0,2,1:T(8,128)}, u32[]{:S(2)}) copy-start(f32[2,1,128]{0,2,1:T(8,128)} %copy.434) | copy-start | bytes 3076
  84.3 21.7 %copy-start.20 = (bf16[128,128]{0,1:T(8,128)(2,1)S(1)}, bf16[128,128]{0,1:T(8,128)(2,1)}, u32[]{:S(2)}) copy-start(bf16[128,128]{0,1:T(8,128)(2,1)} %copy-done.19) | copy-start | bytes 98308
  84.3 22.0 %copy-start.22 = (bf16[128,128]{0,1:T(8,128)(2,1)S(1)}, bf16[128,128]{0,1:T(8,128)(2,1)}, u32[]{:S(2)}) copy-start(bf16[128,128]{0,1:T(8,128)(2,1)} %get-tuple-element.461) | copy-start | bytes 98308
  85.2 22.0 %copy-start.10 = (bf16[256,128]{0,1:T(8,128)(2,1)S(1)}, bf16[256,128]{0,1:T(8,128)(2,1)}, u32[]{:S(2)}) copy-start(bf16[256,128]{0,1:T(8,128)(2,1)} %copy-done.9) | copy-start | bytes 196612
  85.2 23.5 %copy-start.17 = (bf16[128,128]{0,1:T(8,128)(2,1)S(1)}, bf16[128,128]{0,1:T(8,128)(2,1)}, u32[]{:S(2)}) copy-start(bf16[128,128]{0,1:T(8,128)(2,1)} %get-tuple-element.459) | copy-start | bytes 98308
  85.9 23.0 %copy-start.15 = (bf16[128,128]{0,1:T(8,128)(2,1)S(1)}, bf16[128,128]{0,1:T(8,128)(2,1)}, u32[]{:S(2)}) copy-start(bf16[128,128]{0,1:T(8,128)(2,1)} %copy-done.14) | copy-start | bytes 98308
  86.8 15.9 %copy-start.107 = (f32[128,2]{0,1:T(2,128)}, f32[128,2]{0,1:T(2,128)S(1)}, u32[]{:S(2)}) copy-start(f32[128,2]{0,1:T(2,128)S(1)} %copy.358) | copy-start | bytes 3076
  87.7 15.0 %copy-start.105 = (f32[128,2]{0,1:T(2,128)}, f32[128,2]{0,1:T(2,128)S(1)}, u32[]{:S(2)}) copy-start(f32[128,2]{0,1:T(2,128)S(1)} %copy.296) | copy-start | bytes 3076
  88.6 14.0 %copy-start.106 = (f32[128,2]{0,1:T(2,128)}, f32[128,2]{0,1:T(2,128)S(1)}, u32[]{:S(2)}) copy-start(f32[128,2]{0,1:T(2,128)S(1)} %copy.289) | copy-start | bytes 3076
  89.6 13.1 %copy-start.108 = (f32[128,2]{0,1:T(2,128)}, f32[128,2]{0,1:T(2,128)S(1)}, u32[]{:S(2)}) copy-start(f32[128,2]{0,1:T(2,128)S(1)} %copy.351) | copy-start | bytes 3076
  102.7 19.4 %copy-start.34 = (bf16[128,2,64]{0,2,1:T(8,128)(2,1)S(1)}, bf16[128,2,64]{0,2,1:T(8,128)(2,1)}, u32[]{:S(2)}) copy-start(bf16[128,2,64]{0,2,1:T(8,128)(2,1)} %slice.823) | copy-start | bytes 98308
  103.7 13.5 %copy-start.110 = (f32[128,2]{0,1:T(2,128)S(1)}, f32[128,2]{0,1:T(2,128)}, u32[]{:S(2)}) copy-start(f32[128,2]{0,1:T(2,128)} %get-tuple-element.267) | copy-start | bytes 3076
  103.7 19.5 %copy-start.31 = (bf16[128,2,64]{0,2,1:T(8,128)(2,1)S(1)}, bf16[128,2,64]{0,2,1:T(8,128)(2,1)}, u32[]{:S(2)}) copy-start(bf16[128,2,64]{0,2,1:T(8,128)(2,1)} %slice.822) | copy-start | bytes 98308
  103.7 19.7 %copy-start.30 = (bf16[128,2,64]{0,2,1:T(8,128)(2,1)S(1)}, bf16[128,2,64]{0,2,1:T(8,128)(2,1)}, u32[]{:S(2)}) copy-start(bf16[128,2,64]{0,2,1:T(8,128)(2,1)} %slice.831) | copy-start | bytes 98308
  104.4 12.9 %copy-start.104 = (f32[2]{0:T(128)S(1)}, f32[2]{0:T(128)}, u32[]{:S(2)}) copy-start(f32[2]{0:T(128)} %get-tuple-element.449) | copy-start | bytes 28
  104.4 14.9 %copy-start.109 = (f32[128,2]{0,1:T(2,128)S(1)}, f32[128,2]{0,1:T(2,128)}, u32[]{:S(2)}) copy-start(f32[128,2]{0,1:T(2,128)} %get-tuple-element.268) | copy-start | bytes 3076
  104.4 15.0 %copy-start.103 = (f32[2]{0:T(128)S(1)}, f32[2]{0:T(128)}, u32[]{:S(2)}) copy-start(f32[2]{0:T(128)} %get-tuple-element.454) | copy-start | bytes 28
  105.8 18.6 %copy-start.28 = (bf16[128,2,64]{0,2,1:T(8,128)(2,1)S(1)}, bf16[128,2,64]{0,2,1:T(8,128)(2,1)}, u32[]{:S(2)}) copy-start(bf16[128,2,64]{0,2,1:T(8,128)(2,1)} %slice.833) | copy-start | bytes 98308
  108.9 15.7 %copy-start.12 = (f32[2,64,64]{2,1,0:T(8,128)}, f32[2,64,64]{2,1,0:T(8,128)S(1)}, u32[]{:S(2)}) copy-start(f32[2,64,64]{2,1,0:T(8,128)S(1)} %convolution_add_fusion.4) | copy-start | bytes 98308
  113.8 20.2 %copy-start.91 = (f32[2]{0:T(128)}, f32[2]{0:T(128)S(1)}, u32[]{:S(2)}) copy-start(f32[2]{0:T(128)S(1)} %get-tuple-element.522) | copy-start | bytes 28
  122.3 12.2 %copy-start.121 = (f32[2]{0:T(128)S(1)}, f32[2]{0:T(128)}, u32[]{:S(2)}) copy-start(f32[2]{0:T(128)} %copy-done.120) | copy-start | bytes 28
  122.3 12.2 %copy-start.130 = (f32[2]{0:T(128)S(1)}, f32[2]{0:T(128)}, u32[]{:S(2)}) copy-start(f32[2]{0:T(128)} %copy-done.129) | copy-start | bytes 28
  127.0 40.6 %copy-start.92 = (f32[2]{0:T(128)}, f32[2]{0:T(128)S(1)}, u32[]{:S(2)}) copy-start(f32[2]{0:T(128)S(1)} %get-tuple-element.528) | copy-start | bytes 28
  153.7 28.9 %copy-start.71 = (f32[1,2,64]{2,1,0:T(2,128)}, f32[1,2,64]{2,1,0:T(2,128)S(1)}, u32[]{:S(2)}) copy-start(f32[1,2,64]{2,1,0:T(2,128)S(1)} %copy.316) | copy-start | bytes 1540
  153.8 28.8 %copy-start.72 = (f32[1,2,64]{2,1,0:T(2,128)}, f32[1,2,64]{2,1,0:T(2,128)S(1)}, u32[]{:S(2)}) copy-start(f32[1,2,64]{2,1,0:T(2,128)S(1)} %copy.318) | copy-start | bytes 1540
  251.7 13.9 %copy-start.29 = (bf16[128,2,64]{0,2,1:T(8,128)(2,1)S(1)}, bf16[128,2,64]{0,2,1:T(8,128)(2,1)}, u32[]{:S(2)}) copy-start(bf16[128,2,64]{0,2,1:T(8,128)(2,1)} %slice.833) | copy-start | bytes 98308
  251.7 13.9 %copy-start.33 = (bf16[128,2,64]{0,2,1:T(8,128)(2,1)S(1)}, bf16[128,2,64]{0,2,1:T(8,128)(2,1)}, u32[]{:S(2)}) copy-start(bf16[128,2,64]{0,2,1:T(8,128)(2,1)} %slice.832) | copy-start | bytes 98308
  257.3 13.8 %copy-start.36 = (bf16[256,2,64]{0,2,1:T(8,128)(2,1)S(1)}, bf16[256,2,64]{0,2,1:T(8,128)(2,1)}, u32[]{:S(2)}) copy-start(bf16[256,2,64]{0,2,1:T(8,128)(2,1)} %rev.16) | copy-start | bytes 196612
  258.1 15.7 %copy-start.39 = (bf16[128,2,64]{0,2,1:T(8,128)(2,1)S(1)}, bf16[128,2,64]{0,2,1:T(8,128)(2,1)}, u32[]{:S(2)}) copy-start(bf16[128,2,64]{0,2,1:T(8,128)(2,1)} %copy-done.38) | copy-start | bytes 98308
  258.1 17.6 %copy-start.49 = (f32[1,128,64]{2,1,0:T(8,128)S(1)}, f32[1,128,64]{2,1,0:T(8,128)}, u32[]{:S(2)}) copy-start(f32[1,128,64]{2,1,0:T(8,128)} %copy.490) | copy-start | bytes 98308
  261.8 15.9 %copy-start.23 = (bf16[128,128]{0,1:T(8,128)(2,1)S(1)}, bf16[128,128]{0,1:T(8,128)(2,1)}, u32[]{:S(2)}) copy-start(bf16[128,128]{0,1:T(8,128)(2,1)} %get-tuple-element.461) | copy-start | bytes 98308
  261.8 15.9 %copy-start.25 = (bf16[128,128]{0,1:T(8,128)(2,1)S(1)}, bf16[128,128]{0,1:T(8,128)(2,1)}, u32[]{:S(2)}) copy-start(bf16[128,128]{0,1:T(8,128)(2,1)} %copy-done.24) | copy-start | bytes 98308
  264.0 15.5 %copy-start.21 = (bf16[128,128]{0,1:T(8,128)(2,1)S(1)}, bf16[128,128]{0,1:T(8,128)(2,1)}, u32[]{:S(2)}) copy-start(bf16[128,128]{0,1:T(8,128)(2,1)} %copy-done.19) | copy-start | bytes 98308
  264.0 15.5 %copy-start.27 = (bf16[128,128]{0,1:T(8,128)(2,1)S(1)}, bf16[128,128]{0,1:T(8,128)(2,1)}, u32[]{:S(2)}) copy-start(bf16[128,128]{0,1:T(8,128)(2,1)} %copy-done.26) | copy-start | bytes 98308
  265.6 15.5 %copy-start.41 = (f32[8,1,64]{2,0,1:T(8,128)S(1)}, f32[8,1,64]{2,0,1:T(8,128)}, u32[]{:S(2)}) copy-start(f32[8,1,64]{2,0,1:T(8,128)} %copy.497) | copy-start | bytes 6148
  266.6 17.9 %copy-start.11 = (bf16[256,128]{0,1:T(8,128)(2,1)S(1)}, bf16[256,128]{0,1:T(8,128)(2,1)}, u32[]{:S(2)}) copy-start(bf16[256,128]{0,1:T(8,128)(2,1)} %copy-done.9) | copy-start | bytes 196612
  266.6 18.8 %copy-start.18 = (bf16[128,128]{0,1:T(8,128)(2,1)S(1)}, bf16[128,128]{0,1:T(8,128)(2,1)}, u32[]{:S(2)}) copy-start(bf16[128,128]{0,1:T(8,128)(2,1)} %get-tuple-element.459) | copy-start | bytes 98308
  270.1 15.5 %copy-start.16 = (bf16[128,128]{0,1:T(8,128)(2,1)S(1)}, bf16[128,128]{0,1:T(8,128)(2,1)}, u32[]{:S(2)}) copy-start(bf16[128,128]{0,1:T(8,128)(2,1)} %copy-done.14) | copy-start | bytes 98308
  272.9 13.6 %copy-start.13 = (f32[2,64,64]{2,1,0:T(8,128)S(1)}, f32[2,64,64]{2,1,0:T(8,128)}, u32[]{:S(2)}) copy-start(f32[2,64,64]{2,1,0:T(8,128)} %copy-done.12) | copy-start | bytes 98308
  274.7 12.7 %copy-start.43 = (f32[1,128,64]{2,1,0:T(8,128)S(1)}, f32[1,128,64]{2,1,0:T(8,128)}, u32[]{:S(2)}) copy-start(f32[1,128,64]{2,1,0:T(8,128)} %copy.476) | copy-start | bytes 98308
  274.7 12.7 %copy-start.44 = (f32[1,128,64]{2,1,0:T(8,128)S(1)}, f32[1,128,64]{2,1,0:T(8,128)}, u32[]{:S(2)}) copy-start(f32[1,128,64]{2,1,0:T(8,128)} %copy.477) | copy-start | bytes 98308
  274.7 12.7 %copy-start.45 = (f32[1,128,64]{2,1,0:T(8,128)S(1)}, f32[1,128,64]{2,1,0:T(8,128)}, u32[]{:S(2)}) copy-start(f32[1,128,64]{2,1,0:T(8,128)} %copy.472) | copy-start | bytes 98308
  274.7 12.7 %copy-start.46 = (f32[1,128,64]{2,1,0:T(8,128)S(1)}, f32[1,128,64]{2,1,0:T(8,128)}, u32[]{:S(2)}) copy-start(f32[1,128,64]{2,1,0:T(8,128)} %copy.475) | copy-start | bytes 98308
  274.7 12.7 %copy-start.47 = (f32[1,128,64]{2,1,0:T(8,128)S(1)}, f32[1,128,64]{2,1,0:T(8,128)}, u32[]{:S(2)}) copy-start(f32[1,128,64]{2,1,0:T(8,128)} %copy.474) | copy-start | bytes 98308
  274.7 12.7 %copy-start.48 = (f32[1,128,64]{2,1,0:T(8,128)S(1)}, f32[1,128,64]{2,1,0:T(8,128)}, u32[]{:S(2)}) copy-start(f32[1,128,64]{2,1,0:T(8,128)} %copy.473) | copy-start | bytes 98308
  274.7 12.7 %copy-start.83 = (f32[2]{0:T(128)S(1)}, f32[2]{0:T(128)}, u32[]{:S(2)}) copy-start(f32[2]{0:T(128)} %copy-done.82) | copy-start | bytes 28
  290.0 51.4 %all-to-all-start.1 = ((bf16[4,64,128]{2,1,0:T(8,128)(2,1)}), bf16[4,64,128]{2,1,0:T(8,128)(2,1)}, u32[]{:S(2)}, u32[]{:S(2)}) async-start(bf16[4,64,128]{2,1,0:T(8,128)(2,1)} %bitcast.230), calls=%async_computation.1 | async-start | bytes 131072 | tf_op jit(solution)/shard_map/all_to_all | solution.py:394
  341.4 10.3 %all-to-all-start.2 = ((bf16[4,64,128]{2,1,0:T(8,128)(2,1)}), bf16[4,64,128]{2,1,0:T(8,128)(2,1)S(1)}, u32[]{:S(2)}, u32[]{:S(2)}) async-start(bf16[4,64,128]{2,1,0:T(8,128)(2,1)} %copy.492), calls=%async_computation.2 | async-start | bytes 131072 | tf_op jit(solution)/shard_map/all_to_all | solution.py:395
  (87 other events, 519.4 us)
Sparse Core Ops, SparseCore 0:
  86.0 87.1 all-gather.13
where the time goes:
time: 365 us; the launch traced here: 361 us
  local copies, waits for them, and re-layouts  116 us (32%)
  blocking collectives  84.2 us (23%)
  matrix products  66.9 us (18%)
  other arithmetic  52.6 us (14%)
  between operations  15.5 us (4%)
  starting transfers between devices  13.1 us (4%)
  waiting for transfers between devices  12.2 us (3%)
    all_gather x6, blocking collectives, collected_together(): both, at, found = (lax.all_gather(jnp.concatenate(lines), axis), 0, {})  84.2 us
    squeeze x28, local copies, waits for them, and re-layouts, prefix_by_axis(): subtotal = combine(subtotal, jax.tree.map(lambda part: part[k], pieces))  20.3 us
    dot_general x8, matrix products, one_block(): jnp.dot(latent_block, key_weight, preferred_element_type=jnp.float32)  13.7 us
    slice x40, local copies, waits for them, and re-layouts, prefix_by_axis(): subtotal = combine(subtotal, jax.tree.map(lambda part: part[k], pieces))  11.3 us
    dot_general x6, matrix products, project(): return jnp.dot(normed, weight_matrix, preferred_element_type=jnp.float32)  9.24 us
    unnamed x307, local copies, waits for them, and re-layouts  9.15 us
    all_to_all x1, waiting for transfers between devices, copy_for_each(): lax.all_to_all(jnp.broadcast_to(value[None], (length, *value.shape)), axi...  7.81 us
    slice x3, local copies, waits for them, and re-layouts, side_by_side(): finished.append(lax.slice_in_dim(out, at, at + a.shape[along], axis=along))  7.65 us
  transfers between devices with their start and end apart: 4, of which 2 were waited for; matrix products, arithmetic and copies ran while one was open for 47% of the time, Pallas kernels for 0%

commit v1 on v0

v1 whole, which is shorter than its diff:
```python
import functools

import jax
import jax.numpy as jnp
from jax import lax
from jax.experimental import pallas as pl
from jax.experimental.pallas import tpu as pltpu
from jax.sharding import Mesh
from jax.sharding import PartitionSpec as P

D = 2048
NOPE = 64
ROPE = 32
ROWS = 64
BLOCK = 256
QR = 384
KVR = 256
SP = ("sp_0", "sp_1", "sp_2")
SP_TP = ("sp_0", "sp_1", "sp_2", "tp")
EPSILON = 1e-06
ROPE_BASE = 10000.0
FLOOR_LOG = -1e30
BF = jnp.bfloat16
F32 = jnp.float32
MESH = pl.DeviceIdType.MESH
HI = lax.Precision.HIGHEST
KCHUNK = 1024


def dot(a, b, precision=None):
    return lax.dot_general(a, b, (((1,), (0,)), ((), ())), precision=precision, preferred_element_type=F32)


def dot_nt(a, b, precision=None):
    return lax.dot_general(a, b, (((1,), (1,)), ((), ())), precision=precision, preferred_element_type=F32)


def lanes(shape):
    return lax.broadcasted_iota(jnp.int32, shape, len(shape) - 1)


def rcopy(src, dst, send_sem, recv_sem, device):
    return pltpu.make_async_remote_copy(
        src_ref=src, dst_ref=dst, send_sem=send_sem, recv_sem=recv_sem, device_id=device, device_id_type=MESH
    )


def rms(v):
    return v * lax.rsqrt(jnp.mean(v * v, axis=-1, keepdims=True) + EPSILON)


def kernel(
    nz, nx, ny,
    tok, gain, hmq, hmk, hmv, hmo, hgt, goff, mng, hqd, qdg, hld, lg, hrt, hqt, hlup,
    cq, sq, cr, sr, kg, hwm, hwa,
    out,
    mq, mk, mv, mo, gt, qd, ld, rt, qt, lup, wm, wa,
    rt4, wqt, normed, ksend, kgot, kvg, psend, qsend, qg, pa, rtot, pb,
    qop, kop, vop, osend, po, fsend, fx, lhs_m, lhs_a,
    w_sem, n_ss, n_rs, g_ss, g_rs, p_ss, p_rs, q_ss, q_rs, a_ss, a_rs, b_ss, b_rs,
    u_ss, u_rs, d_ss, d_rs, o_ss, o_rs, f_ss, f_rs,
):
    z = lax.axis_index("sp_0")
    x = lax.axis_index("sp_1")
    c = lax.axis_index("sp_2")
    y = lax.axis_index("tp")
    nr = nx * 2
    me = x * 2 + c

    def at_y(d):
        return {"tp": lax.rem(y + d, ny)}

    def at_row(d):
        j = lax.rem(me + d, nr)
        return {"sp_1": j // 2, "sp_2": lax.rem(j, 2)}

    def at_z(d):
        return {"sp_0": lax.rem(z + d, nz)}

    pairs = ((hqd, qd), (hld, ld), (hrt, rt), (hqt, qt), (hlup, lup), (hmq, mq), (hmk, mk), (hmv, mv),
             (hmo, mo), (hgt, gt), (hwm, wm), (hwa, wa))
    loads = [pltpu.make_async_copy(a, b, w_sem.at[i]) for i, (a, b) in enumerate(pairs)]
    for load in loads:
        load.start()

    barrier = pltpu.get_barrier_semaphore()
    peers = [at_y(d) for d in range(1, ny)] + [at_row(d) for d in range(1, nr)] + [at_z(d) for d in range(1, nz)]
    for peer in peers:
        pl.semaphore_signal(barrier, inc=1, device_id=peer, device_id_type=MESH)

    xt = tok[...].astype(F32)
    normed_local = (rms(xt) * gain[...]).astype(BF)
    normed[pl.ds(y, 1)] = normed_local[None]
    pl.semaphore_wait(barrier, len(peers))
    n_copies = [rcopy(normed.at[y], normed.at[y], n_ss.at[d], n_rs.at[d], at_y(d)) for d in range(1, ny)]
    for copy in n_copies:
        copy.start()

    loads[0].wait()
    loads[1].wait()
    ql = (rms(dot(normed_local, qd[...])) * qdg[...]).astype(BF)
    la = (rms(dot(normed_local, ld[...])) * lg[...]).astype(BF)
    loads[2].wait()
    for i in range(4):
        rt4[pl.ds(32 * i, 32), :] = rt[...]
        rt4[pl.ds(128 + 32 * i, 16), :] = rt[pl.ds(16, 16), :]
        rt4[pl.ds(128 + 32 * i + 16, 16), :] = rt[pl.ds(0, 16), :]
    ro = dot_nt(normed_local, rt4[...])
    ra, rb = ro[:, :128], ro[:, 128:]
    rscale = lax.rsqrt(jnp.mean(ra * ra, axis=-1, keepdims=True) + EPSILON)
    lane = lanes((ROWS, 128))
    rot = (ra * rscale) * cr[...] + (rb * rscale) * sr[...]
    rot = jnp.where(lane // ROPE == y, rot, 0.0).astype(BF)
    loads[3].wait()
    for h in range(8):
        wqt[pl.ds(128 * h, 96), :] = qt[pl.ds(96 * h, 96), :]
        wqt[pl.ds(128 * h + 96, 16), :] = qt[pl.ds(96 * h + 80, 16), :]
        wqt[pl.ds(128 * h + 112, 16), :] = qt[pl.ds(96 * h + 64, 16), :]
    loads[4].wait()
    qall = dot_nt(ql, wqt[...])
    kvall = dot(la, lup[...])
    for h in range(8):
        q = qall[:, 128 * h : 128 * h + 128]
        q2 = q * q
        mp = jnp.sum(jnp.where(lane < NOPE, q2, 0.0), axis=-1, keepdims=True) * (1.0 / NOPE)
        mr = jnp.sum(jnp.where(lane >= 96, q2, 0.0), axis=-1, keepdims=True) * (1.0 / ROPE)
        qn = q * jnp.where(lane < NOPE, lax.rsqrt(mp + EPSILON), lax.rsqrt(mr + EPSILON))
        qv = (qn * cq[...] + pltpu.roll(qn, 96, 1) * sq[...]).astype(BF)
        kv = kvall[:, 128 * h : 128 * h + 128]
        mp = jnp.sum(jnp.where(lane < NOPE, kv * kv, 0.0), axis=-1, keepdims=True) * (1.0 / NOPE)
        kvv = (kv * jnp.where(lane < NOPE, lax.rsqrt(mp + EPSILON) * kg[...], 1.0)).astype(BF)
        j = h // 2
        o = (h % 2) * 128
        ksend[j, :, o : o + 128] = kvv
        ksend[j, :, 256 + o : 384 + o] = qv
    for j in range(ny):
        ksend[j, :, 512:640] = rot
    k_copies = [rcopy(ksend.at[lax.rem(y + d, ny)], kgot.at[y], g_ss.at[d], g_rs.at[d], at_y(d)) for d in range(1, ny)]
    for copy in k_copies:
        copy.start()
    kgot[pl.ds(y, 1)] = ksend[pl.ds(y, 1)]

    for copy in n_copies:
        copy.wait_recv()
    for i in range(5, 10):
        loads[i].wait()
    rows = normed[...].reshape(BLOCK, D)
    mem_q = dot(rows, mq[...]).astype(BF)
    mem_k = (dot(rows, mk[...]) * 0.125).astype(BF)
    mem_v = dot(rows, mv[...]).astype(BF)
    gate_t = dot_nt(gt[...], rows).astype(BF)

    for copy in k_copies:
        copy.wait_recv()
    got = kgot[...].reshape(BLOCK, 640)
    first = c == 0
    rsum = (
        (kgot[0, :, 512:640].astype(F32) + kgot[1, :, 512:640].astype(F32))
        + (kgot[2, :, 512:640].astype(F32) + kgot[3, :, 512:640].astype(F32))
    ).astype(BF)
    h0, h1 = got[:, 0:128], got[:, 128:256]
    psend[pl.ds(0, BLOCK), :] = jnp.where(first, h1, h0)
    psend[pl.ds(BLOCK, ROWS), :] = rsum
    p_copy = rcopy(psend, kvg.at[z, c], p_ss, p_rs, {"sp_2": 1 - c})
    p_copy.start()
    qsend[0] = got[:, 256:384]
    qsend[1] = got[:, 384:512]
    q_copies = []
    for d in range(1, nr):
        j = lax.rem(me + d, nr)
        copy = rcopy(qsend.at[lax.rem(j, 2)], qg.at[me], q_ss.at[d], q_rs.at[d], at_row(d))
        copy.start()
        q_copies.append(copy)
    kvg[pl.ds(z, 1), pl.ds(c, 1), pl.ds(0, BLOCK), :] = jnp.where(first, h0, h1)[None, None]
    kvg[pl.ds(z, 1), pl.ds(c, 1), pl.ds(BLOCK, ROWS), :] = rsum[None, None]
    qg[pl.ds(me, 1)] = qsend[pl.ds(c, 1)]

    up, down = {}, {}

    def ring_step(s):
        for half in range(2):
            if s <= nz // 2 - 1 or half == 0:
                chunk = lax.rem(z - (s - 1) + nz, nz)
                copy = rcopy(kvg.at[chunk, half], kvg.at[chunk, half], u_ss.at[s, half], u_rs.at[s, half], at_z(1))
                copy.start()
                up[s, half] = copy
            if s <= nz // 2 - 1 or half == 1:
                chunk = lax.rem(z + (s - 1), nz)
                copy = rcopy(kvg.at[chunk, half], kvg.at[chunk, half], d_ss.at[s, half], d_rs.at[s, half], at_z(nz - 1))
                copy.start()
                down[s, half] = copy

    def ring_wait(s):
        for half in range(2):
            if (s, half) in up:
                up[s, half].wait_recv()
            if (s, half) in down:
                down[s, half].wait_recv()

    lane2 = lanes((BLOCK, 128))
    low = lane2 < 64
    row8 = lax.broadcasted_iota(jnp.int32, (8, 32), 0)
    col8 = lax.broadcasted_iota(jnp.int32, (8, 32), 1)
    pick = (col8 == (row8 // 2) * 8 + y * 2 + lax.rem(row8, 2)).astype(BF)
    pre = dot(pick, gate_t) + goff[...]
    low_t = lax.broadcasted_iota(jnp.int32, (128, BLOCK), 0) < 64

    def spread(r0, r1):
        wide = jnp.where(low_t, jnp.broadcast_to(r0, (128, BLOCK)), jnp.broadcast_to(r1, (128, BLOCK)))
        return jnp.transpose(wide)

    log_f = jnp.minimum(pre, 0.0) - jnp.log1p(jnp.exp(-jnp.abs(pre)))
    ti = lax.broadcasted_iota(jnp.int32, (BLOCK, BLOCK), 0)
    si = lax.broadcasted_iota(jnp.int32, (BLOCK, BLOCK), 1)
    masks = (si <= ti, si >= ti)
    zero = jnp.zeros_like(mem_q)
    s_heads = (dot_nt(jnp.where(low, mem_q, zero), mem_k), dot_nt(jnp.where(low, zero, mem_q), mem_k))
    v_f = mem_v.astype(F32)
    k_f = mem_k.astype(F32)
    q_f = mem_q.astype(F32)
    parts = []
    for way in range(2):
        i_wide = spread(pre[4 * way : 4 * way + 1], pre[4 * way + 1 : 4 * way + 2])
        f_wide = spread(log_f[4 * way + 2 : 4 * way + 3], log_f[4 * way + 3 : 4 * way + 4])
        cum = dot(masks[way].astype(F32), f_wide, HI)
        g = i_wide - cum
        g_t = jnp.transpose(g)
        nums, dens, tops = [], [], []
        for h in range(2):
            decay = cum[:, 64 * h : 64 * h + 1] + g_t[64 * h : 64 * h + 1, :]
            decay = jnp.where(masks[way], decay, -jnp.inf)
            top = jnp.max(decay, axis=-1, keepdims=True)
            w = s_heads[h] * jnp.exp(decay - top)
            dens.append(jnp.sum(w, axis=-1, keepdims=True))
            nums.append(dot(w.astype(BF), mem_v))
            tops.append(top)
        num = jnp.where(low, nums[0], nums[1])
        den = jnp.where(low, dens[0], dens[1])
        top = jnp.where(low, tops[0], tops[1])
        total = jnp.sum(f_wide, axis=0, keepdims=True)
        growth = total + g
        level = jnp.max(growth, axis=0, keepdims=True)
        inflow = jnp.exp(growth - level)
        mat = lax.dot_general(
            inflow * v_f, k_f, (((0,), (0,)), ((), ())), precision=HI, preferred_element_type=F32
        )
        fold = jnp.where(lanes((64, 128)) < 64, mat[:64], mat[64:])
        normal = jnp.sum(inflow * k_f, axis=0, keepdims=True)
        pa[pl.ds(me, 1), way, pl.ds(0, 64), :] = fold[None]
        pa[pl.ds(me, 1), way, pl.ds(64, 8), :] = jnp.concatenate(
            [normal, level, total, jnp.zeros((5, 128), F32)], axis=0
        )[None]
        parts.append((num, den, top, cum))
    a_copies = [rcopy(pa.at[me], pa.at[me], a_ss.at[d], a_rs.at[d], at_row(d)) for d in range(1, nr)]
    for copy in a_copies:
        copy.start()
    p_copy.wait_recv()
    ring_step(1)
    out_gate = jax.nn.sigmoid(dot(rows, mo[...]).astype(BF).astype(F32))

    for copy in a_copies:
        copy.wait_recv()

    def gather_levels(get, count, order, valid, running):
        found = []
        for j in order:
            vec = get(j)
            ok = valid(j)
            found.append((j, ok, jnp.where(ok, vec[1:2] + running, FLOOR_LOG)))
            running = running + jnp.where(ok, vec[2:3], 0.0)
        return found, running

    def merge(entries):
        joined = entries[0][2]
        for _, _, level in entries[1:]:
            joined = jnp.maximum(joined, level)
        mat = jnp.zeros((72, 128), F32)
        for fetch, ok, level in entries:
            scale = jnp.where(ok, jnp.exp(level - joined), 0.0)
            mat = mat + jnp.where(ok, fetch(), 0.0) * scale
        return mat, joined

    def row_vec(way):
        return lambda j: pa[j, way, pl.ds(64, 8), :]

    def row_mat(way, j):
        return lambda: pa[j, way]

    orders = (list(reversed(range(nr))), list(range(nr)))
    z_orders = (list(reversed(range(nz))), list(range(nz)))
    for way in range(2):
        found, total = gather_levels(row_vec(way), nr, orders[way], lambda j: j >= 0, jnp.zeros((1, 128), F32))
        mat, joined = merge([(row_mat(way, j), ok, level) for j, ok, level in found])
        rtot[way, pl.ds(0, 64), :] = mat[:64]
        rtot[way, pl.ds(64, 8), :] = jnp.concatenate(
            [mat[64:65], joined, total, jnp.zeros((5, 128), F32)], axis=0
        )
    b_copies = []
    for d in range(1, nz):
        wrapped = (z + d) // nz
        copy = rcopy(rtot.at[wrapped], pb.at[z], b_ss.at[d], b_rs.at[d], at_z(d))
        copy.start()
        b_copies.append(copy)
    pb[pl.ds(z, 1)] = jnp.zeros((1, 72, 128), F32)
    ring_wait(1)
    ring_step(2)
    for copy in b_copies:
        copy.wait_recv()

    hsum = jnp.zeros((BLOCK, 128), F32)
    bi = lax.broadcasted_iota(jnp.int32, (128, 128), 0) // 64
    bj = lax.broadcasted_iota(jnp.int32, (128, 128), 1) // 64
    ones_block = (bi == bj).astype(F32)
    for way in range(2):
        if way == 0:
            ok_row, ok_z = (lambda j: j < me), (lambda j: j < z)
        else:
            ok_row, ok_z = (lambda j: j > me), (lambda j: j > z)
        found, running = gather_levels(row_vec(way), nr, orders[way], ok_row, jnp.zeros((1, 128), F32))
        entries = [(row_mat(way, j), ok, level) for j, ok, level in found]
        found, _ = gather_levels(lambda j: pb[j, pl.ds(64, 8), :], nz, z_orders[way], ok_z, running)
        entries += [((lambda j: (lambda: pb[j]))(j), ok, level) for j, ok, level in found]
        mat, level = merge(entries)
        fold, normal = mat[:64], mat[64:65]
        low64 = lanes((64, 128)) < 64
        full = jnp.concatenate([jnp.where(low64, fold, 0.0), jnp.where(low64, 0.0, fold)], axis=0)
        num, den, top, cum = parts[way]
        carried_log = cum + level
        joined = jnp.maximum(top, carried_log)
        own = jnp.exp(top - joined)
        carried = jnp.exp(carried_log - joined)
        num = num * own + carried * dot_nt(q_f, full, HI)
        den = den * own + carried * dot(q_f * normal, ones_block, HI)
        hsum = hsum + num / jnp.maximum(jnp.abs(den), jnp.exp(-joined))
    mean = dot(hsum * hsum, ones_block, HI) * (1.0 / 64)
    combined = hsum * lax.rsqrt(mean + EPSILON) * mng[pl.ds(y, 1), :]
    mem_rows = (combined * out_gate).astype(BF)
    for j in range(ny):
        fsend[j, :, 0:128] = mem_rows[64 * j : 64 * j + 64]

    for copy in q_copies:
        copy.wait_recv()
    ring_wait(2)
    ring_step(3)
    tile_r = lax.broadcasted_iota(jnp.int32, (128, 128), 0)
    tile_c = lax.broadcasted_iota(jnp.int32, (128, 128), 1)
    tile_m = (tile_r == 64 + lax.rem(tile_c, 32)).astype(BF)

    for j in range(nr):
        slab = qg[j]
        qop[j, :, 0:128] = jnp.where(low, slab, jnp.zeros_like(slab))
        qop[j, :, 128:256] = dot(slab, tile_m).astype(BF)
    ring_wait(3)
    ring_step(nz // 2)
    ring_wait(nz // 2)

    def fill(i, carry):
        for half in range(2):
            base = pl.multiple_of(i * 512 + half * 256, 256)
            kvs = kvg[i, half, pl.ds(0, BLOCK), :]
            kop[pl.ds(base, BLOCK), 0:128] = kvs
            vop[pl.ds(base, BLOCK), :] = jnp.where(low, jnp.ones_like(kvs), kvs)
            r = kvg[i, half, pl.ds(BLOCK, ROWS), :]
            for j in range(4):
                kop[pl.ds(base + 64 * j, ROWS), 128:256] = jnp.where(lane // ROPE == j, r, jnp.zeros_like(r))
        return carry

    lax.fori_loop(0, nz, fill, 0)
    n_chunks = nz * 512 // KCHUNK

    def block(i, carry):
        d = lax.rem(i + 1, nr)
        j = lax.rem(me + d, nr)
        qv = qop[j]
        top = jnp.full((BLOCK, 1), FLOOR_LOG, F32)
        acc = jnp.zeros((BLOCK, 128), F32)
        for k in range(n_chunks):
            s = dot_nt(qv, kop[pl.ds(k * KCHUNK, KCHUNK), :])
            new = jnp.maximum(top, jnp.max(s, axis=-1, keepdims=True))
            p = jnp.exp(s - new).astype(BF)
            acc = acc * jnp.exp(top - new) + dot(p, vop[pl.ds(k * KCHUNK, KCHUNK), :])
            top = new
        den = acc[:, 0:1]
        lse = top + jnp.log(den)
        hi = lse.astype(BF).astype(F32)
        mid = (lse - hi).astype(BF).astype(F32)
        lo = (lse - hi) - mid
        msg = jnp.where(lane2 == 0, hi, jnp.where(lane2 == 1, mid, jnp.where(lane2 == 2, lo, acc / den)))
        osend[pl.ds(d, 1)] = msg.astype(BF)[None]

        @pl.when(i < nr - 1)
        def _():
            rcopy(osend.at[d], po.at[me], o_ss.at[d], o_rs.at[d], at_row(d)).start()

        return carry

    lax.fori_loop(0, nr, block, 0)
    po[pl.ds(me, 1)] = osend[pl.ds(0, 1)]
    o_copies = [rcopy(osend.at[d], po.at[me], o_ss.at[d], o_rs.at[d], at_row(d)) for d in range(1, nr)]
    for copy in o_copies:
        copy.wait_recv()
    heads = []
    for h in range(2):
        msgs = [po[2 * j + h].astype(F32) for j in range(nx)]
        lses = [(m[:, 0:1] + m[:, 1:2]) + m[:, 2:3] for m in msgs]
        joined = functools.reduce(jnp.maximum, lses)
        ws = [jnp.exp(v - joined) for v in lses]
        heads.append(sum(w * m for w, m in zip(ws, msgs)) / sum(ws))
    att = jnp.where(low, pltpu.roll(heads[0], 64, 1), heads[1]).astype(BF)
    for j in range(ny):
        fsend[j, :, 128:256] = att[64 * j : 64 * j + 64]

    f_copies = [rcopy(fsend.at[lax.rem(y + d, ny)], fx.at[y], f_ss.at[d], f_rs.at[d], at_y(d)) for d in range(1, ny)]
    for copy in f_copies:
        copy.start()
    fx[pl.ds(y, 1)] = fsend[pl.ds(y, 1)]
    loads[10].wait()
    loads[11].wait()
    for copy in f_copies:
        copy.wait_recv()
    for j in range(ny):
        lhs_m[:, 128 * j : 128 * j + 128] = fx[j, :, 0:128]
        lhs_a[:, 128 * j : 128 * j + 128] = fx[j, :, 128:256]
    out[...] = (dot(lhs_m[...], wm[...]) + dot(lhs_a[...], wa[...])).astype(BF)

    for copies in (n_copies, k_copies, [p_copy], q_copies, a_copies, b_copies, o_copies, f_copies):
        for copy in copies:
            copy.wait_send()
    for copy in list(up.values()) + list(down.values()):
        copy.wait_send()


def tables(segment, member, query_gain, key_gain):
    lane = jnp.arange(128, dtype=jnp.int32)
    positions = segment * BLOCK + member * ROWS + jnp.arange(ROWS, dtype=jnp.int32)
    frequency = ROPE_BASE ** (-(lane % 16).astype(F32) / 16)
    angles = positions.astype(F32)[:, None] * frequency[None, :]
    cosine, sine = jnp.cos(angles), jnp.sin(angles)
    sign = jnp.where(lane % 32 < 16, -1.0, 1.0)
    own = key_gain[NOPE + lane % 32]
    swapped = key_gain[NOPE + (lane + 16) % 32]
    cr = cosine * own
    sr = sine * sign * swapped
    scale = (NOPE + ROPE) ** (-0.5)
    in_rope = (lane >= 64) & (lane < 96)
    q_own = jnp.where(lane < 96, query_gain[jnp.minimum(lane, 95)], 0.0) * scale
    q_swap = query_gain[NOPE + (lane + 16) % 32] * scale
    cq = jnp.where(lane < 64, 1.0, jnp.where(in_rope, cosine, 0.0)) * q_own
    sq = jnp.where(in_rope, sine * sign * q_swap, 0.0)
    kg = key_gain[jnp.minimum(lane, 63)]
    return cq, sq, cr, sr, kg[None, :]


def body(nz, nx, ny, tokens, input_gain, memory_query, memory_key, memory_value, memory_outgate, memory_gates,
         gate_offset, memory_norm_gain, query_down, query_down_gain, latent_down, latent_gain, rotary_down,
         query_up, latent_up, query_gain, key_gain, memory_output, attention_output):
    segment = lax.axis_index(SP)
    member = lax.axis_index("tp")
    cq, sq, cr, sr, kg = tables(segment, member, query_gain, key_gain)
    args = (
        tokens, input_gain.reshape(1, D), memory_query, memory_key, memory_value, memory_outgate,
        jnp.transpose(memory_gates, (1, 2, 0)).reshape(32, D),
        jnp.transpose(gate_offset, (0, 2, 1)).reshape(8, BLOCK),
        memory_norm_gain.reshape(4, 128), query_down, query_down_gain.reshape(1, QR), latent_down,
        latent_gain.reshape(1, KVR), rotary_down.T,
        jnp.transpose(query_up, (1, 2, 0)).reshape(8 * (NOPE + ROPE), QR),
        latent_up.reshape(KVR, 1024), cq, sq, cr, sr, kg, memory_output, attention_output,
    )
    nr = nx * 2
    in_hbm = {2, 3, 4, 5, 6, 9, 11, 13, 14, 15, 21, 22}
    vmem = pl.BlockSpec(memory_space=pltpu.VMEM)
    hbm = pl.BlockSpec(memory_space=pl.ANY)
    dma = pltpu.SemaphoreType.DMA
    keys = nz * 512
    scratch = [
        pltpu.VMEM((D, 128), BF), pltpu.VMEM((D, 128), BF), pltpu.VMEM((D, 128), BF), pltpu.VMEM((D, 128), BF),
        pltpu.VMEM((32, D), BF), pltpu.VMEM((D, QR), BF), pltpu.VMEM((D, KVR), BF), pltpu.VMEM((32, D), BF),
        pltpu.VMEM((768, QR), BF), pltpu.VMEM((KVR, 1024), BF), pltpu.VMEM((512, D), BF), pltpu.VMEM((512, D), BF),
        pltpu.VMEM((256, D), BF), pltpu.VMEM((1024, QR), BF), pltpu.VMEM((ny, ROWS, D), BF),
        pltpu.VMEM((ny, ROWS, 640), BF), pltpu.VMEM((ny, ROWS, 640), BF),
        pltpu.VMEM((nz, 2, BLOCK + ROWS, 128), BF), pltpu.VMEM((BLOCK + ROWS, 128), BF),
        pltpu.VMEM((2, BLOCK, 128), BF), pltpu.VMEM((nr, BLOCK, 128), BF),
        pltpu.VMEM((nr, 2, 72, 128), F32), pltpu.VMEM((2, 72, 128), F32), pltpu.VMEM((nz, 72, 128), F32),
        pltpu.VMEM((nr, BLOCK, 256), BF), pltpu.VMEM((keys, 256), BF), pltpu.VMEM((keys, 128), BF),
        pltpu.VMEM((nr, BLOCK, 128), BF), pltpu.VMEM((nr, BLOCK, 128), BF),
        pltpu.VMEM((ny, ROWS, 256), BF), pltpu.VMEM((ny, ROWS, 256), BF),
        pltpu.VMEM((ROWS, 512), BF), pltpu.VMEM((ROWS, 512), BF),
        dma((12,)), dma((ny,)), dma((ny,)), dma((ny,)), dma((ny,)), dma, dma,
        dma((nr,)), dma((nr,)), dma((nr,)), dma((nr,)), dma((nz,)), dma((nz,)),
        dma((nz // 2 + 1, 2)), dma((nz // 2 + 1, 2)), dma((nz // 2 + 1, 2)), dma((nz // 2 + 1, 2)),
        dma((nr,)), dma((nr,)), dma((ny,)), dma((ny,)),
    ]
    return pl.pallas_call(
        functools.partial(kernel, nz, nx, ny),
        out_shape=jax.ShapeDtypeStruct((ROWS, D), BF),
        in_specs=[hbm if i in in_hbm else vmem for i in range(len(args))],
        out_specs=vmem,
        scratch_shapes=scratch,
        compiler_params=pltpu.CompilerParams(
            collective_id=0, has_side_effects=True, vmem_limit_bytes=60 * 1024 * 1024
        ),
        name="mixer",
    )(*args)


def solution(mesh):
    ny = mesh.shape["tp"]
    nz, nx = 8, 4
    split = Mesh(mesh.devices.reshape(nz, nx, 2, ny), ("sp_0", "sp_1", "sp_2", "tp"))
    rep = P()
    head = P(None, "tp")
    in_specs = (
        P(SP_TP, None), rep, head, head, head, head, rep, P(None, SP, "tp"),
        rep, rep, rep, rep, rep, rep, rep, rep, rep, rep, rep, rep,
    )
    return jax.shard_map(
        functools.partial(body, nz, nx, ny), mesh=split, in_specs=in_specs, out_specs=P(SP_TP, None), check_vma=False
    )
```

time: 365 us -> 101 us (0.28)
  local copies, waits for them, and re-layouts: 116 us -> 11.6 us
  Pallas kernels: 0 us -> 86.4 us
  blocking collectives: 84.2 us -> 0 us
  matrix products: 66.9 us -> 0 us
  other arithmetic: 52.6 us -> 0.91 us
  between operations: 15.5 us -> 0.14 us
  starting transfers between devices: 13.1 us -> 0 us
  waiting for transfers between devices: 12.2 us -> 0 us
    pallas_call x0 -> x1, Pallas kernels: none -> 86.4 us  [body(): pl.pallas_call(functools.partial(kernel, nz, nx, ny), out_shape=jax.Shape...]
    all_gather x6 -> x0, blocking collectives: 84.2 us -> none  [collected_together(): both, at, found = (lax.all_gather(jnp.concatenate(lines), axis), 0, {})]
    dot_general x65 -> x0, matrix products: 66.9 us -> none  [the longest x8 13.7 us: one_block(): jnp.dot(latent_block, key_weight, preferred_element_type=jnp.float32)]
    slice x71 -> x0, local copies, waits for them, and re-layouts: 36 us -> none  [the longest x40 11.3 us: prefix_by_axis(): subtotal = combine(subtotal, jax.tree.map(lambda part: part[k], pieces))]
    squeeze x30 -> x0, local copies, waits for them, and re-layouts: 22.7 us -> none  [the longest x28 20.3 us: prefix_by_axis(): subtotal = combine(subtotal, jax.tree.map(lambda part: part[k], pieces))]
    add x29 -> x0, other arithmetic: 13.1 us -> none  [the longest x6 3.96 us: chain(): scale_early[:, None] * normal_early + scale_late[:, None] * normal_late]
    all_to_all x3 -> x0, starting transfers between devices: 13.1 us -> none  [the longest x1 4.7 us: body(): lax.all_to_all(attention_rows, 'tp', split_axis=0, concat_axis=1, tiled=T...]
    mul x53 -> x0, local copies, waits for them, and re-layouts: 13 us -> none  [the longest x24 5.19 us: chain(): scale_late[:, None, None] * memory_late]
  transfers between devices with their start and end apart: 4 -> 0, of which waited for: 2 -> 0; matrix products, arithmetic and copies ran while one was open for 47% -> 0% of each run, Pallas kernels for 0% -> 0%
where the time goes in v1:
time: 101 us; the launch traced here: 99.1 us
  Pallas kernels  86.4 us (86%)
  local copies, waits for them, and re-layouts  11.6 us (11%)
    pallas_call x1, Pallas kernels, body(): pl.pallas_call(functools.partial(kernel, nz, nx, ny), out_shape=jax.Shape...  86.4 us
    unnamed x10, local copies, waits for them, and re-layouts  2.58 us

profile of v1, /device:TPU:2, one launch (start us, length us, event | category | flops | bytes accessed | tf_op | source)
XLA Modules:
  0.0 99.1 jit_solution(15048091244241950284)
XLA Ops:
  0.0 0.0 copy-start
  0.0 0.0 copy-start.1
  0.0 0.0 copy-start.2
  0.0 0.0 copy-start.3
  0.1 1.4 %reshape.170.qdg = f32[1,384]{1,0:T(1,128)} reshape(f32[384]{0:T(512)} %param.30) | data formatting | bytes 3072 | tf_op jit(solution)/shard_map/reshape | solution.py:464
  1.5 0.0 copy-done
  1.5 1.2 %gather_fusion.3 = f32[128]{0:T(128)S(1)} fusion(f32[96]{0:T(128)S(1)} %copy-done, s32[1024]{0:T(1024)S(1)} %pad_clamp_fusion.2), kind=kCustom, calls=%fused_computation.3 | custom fusion | bytes 1536 | tf_op jit(solution)/shard_map/gather | solution.py:441
  2.7 1.6 %gather_fusion.1 = f32[128]{0:T(128)S(1)} fusion(f32[96]{0:T(128)} %param.36, s32[1024]{0:T(1024)S(1)} %pad_clamp_fusion.2), kind=kCustom, calls=%fused_computation.1 | custom fusion | bytes 1536 | tf_op jit(solution)/shard_map/gather | solution.py:447
  4.3 1.2 %gather_fusion.2 = f32[128]{0:T(128)S(1)} fusion(f32[96]{0:T(128)S(1)} %copy-done, s32[1024]{0:T(1024)S(1)} %pad_clamp_fusion.1), kind=kCustom, calls=%fused_computation.2 | custom fusion | bytes 1536 | tf_op jit(solution)/shard_map/gather | solution.py:440
  5.6 1.8 %gather_fusion.4 = f32[128]{0:T(128)} fusion(f32[96]{0:T(128)S(1)} %copy-done, s32[1024]{0:T(1024)S(1)} %pad_clamp_fusion), kind=kCustom, calls=%fused_computation.4 | custom fusion | bytes 1536 | tf_op jit(solution)/shard_map/gather | solution.py:450
  7.4 0.0 copy-done.1
  7.4 1.2 %gather_fusion = f32[128]{0:T(128)S(1)} fusion(f32[96]{0:T(128)S(1)} %copy-done.1, s32[1024]{0:T(1024)S(1)} %pad_clamp_fusion.3), kind=kCustom, calls=%fused_computation | custom fusion | bytes 1536 | tf_op jit(solution)/shard_map/gather | solution.py:446
  8.6 0.0 copy-done.3
  8.6 0.6 reshape.168.goff
  9.3 0.8 fusion.5
  10.1 0.0 copy-done.2
  10.1 0.9 copy.23
  11.0 86.4 %mixer.1 = bf16[64,2048]{1,0:T(8,128)(2,1)} custom-call(bf16[64,2048]{1,0:T(8,128)(2,1)} %tok.1, f32[1,2048]{1,0:T(1,128)} %bitcast.30, bf16[2048,128]{1,0:T(8,128)(2,1)} %hmq.1, bf16[2048,128]{1,0:T(8,128)(2,1)} %hmk.1, bf16[2048,128]{1,0:T(8,128)(2,1)} %hmv.1, bf16[2048,128]{1,0:T(8,128)(2,1)} %hmo.1, bf16[32,2048]{1,0:T(8,128)(2,1)} %bitcast.27, ...), custom_call_target="tpu_custom_call" | custom-call | tf_op jit(solution)/shard_map/mixer/pallas_call | solution.py:493
  97.4 1.7 %copy.25 = bf16[64,2048]{1,0:T(8,128)(2,1)} copy(bf16[64,2048]{1,0:T(8,128)(2,1)} %mixer.1) | data formatting | bytes 524288
  (12 shorter events, 0.1 us)
Async XLA Ops:
  0.0 1.5 %copy-start = (f32[96]{0:T(128)S(1)}, f32[96]{0:T(128)}, u32[]{:S(2)}) copy-start(f32[96]{0:T(128)} %param.37) | copy-start | bytes 1156
  0.0 7.4 %copy-start.1 = (f32[96]{0:T(128)S(1)}, f32[96]{0:T(128)}, u32[]{:S(2)}) copy-start(f32[96]{0:T(128)} %param.36) | copy-start | bytes 1156
  0.0 10.1 %copy-start.2 = (bf16[256,8,128]{2,1,0:T(8,128)(2,1)S(1)}, bf16[256,8,128]{2,1,0:T(8,128)(2,1)}, u32[]{:S(2)}) copy-start(bf16[256,8,128]{2,1,0:T(8,128)(2,1)} %param.35) | copy-start | bytes 1572868
  0.0 8.6 %copy-start.3 = (f32[4,256,2]{1,2,0:T(2,128)S(1)}, f32[4,256,2]{1,2,0:T(2,128)}, u32[]{:S(2)}) copy-start(f32[4,256,2]{1,2,0:T(2,128)} %param.27) | copy-start | bytes 24580

commit v2 on v1

v2 whole, which is shorter than its diff:
```python
import functools

import jax
import jax.numpy as jnp
from jax import lax
from jax.experimental import pallas as pl
from jax.experimental.pallas import tpu as pltpu
from jax.sharding import Mesh
from jax.sharding import PartitionSpec as P

D = 2048
NOPE = 64
ROPE = 32
ROWS = 64
BLOCK = 256
QR = 384
KVR = 256
SP = ("sp_0", "sp_1", "sp_2")
SP_TP = ("sp_0", "sp_1", "sp_2", "tp")
EPSILON = 1e-06
ROPE_BASE = 10000.0
FLOOR_LOG = -1e30
BF = jnp.bfloat16
F32 = jnp.float32
MESH = pl.DeviceIdType.MESH
HI = lax.Precision.HIGHEST
FREQUENCIES = [float(ROPE_BASE ** (-j / 16)) for j in range(16)]


def dot(a, b, precision=None):
    return lax.dot_general(a, b, (((1,), (0,)), ((), ())), precision=precision, preferred_element_type=F32)


def dot_nt(a, b, precision=None):
    return lax.dot_general(a, b, (((1,), (1,)), ((), ())), precision=precision, preferred_element_type=F32)


def lanes(shape):
    return lax.broadcasted_iota(jnp.int32, shape, len(shape) - 1)


def rcopy(src, dst, send_sem, recv_sem, device):
    return pltpu.make_async_remote_copy(
        src_ref=src, dst_ref=dst, send_sem=send_sem, recv_sem=recv_sem, device_id=device, device_id_type=MESH
    )


def rms(v):
    return v * lax.rsqrt(jnp.mean(v * v, axis=-1, keepdims=True) + EPSILON)


def kernel(
    nz, nx, ny,
    tok, gain, hmq, hmk, hmv, hmo, hgt, goff, mng, hqd, qdg, hld, lg, hrt, hqt, hlup,
    qgain, kgain, hwm, hwa,
    out,
    mq, mk, mv, mo, gt, qd, ld, rt, qt, lup, wm, wa,
    rt4, wqt, lupf, trig, normed, ebuf, kvg, psend, qsend, qg, asend, agot, rtot, pb, csend, cgot,
    qop, kop, vt, acc_s, top_s, osend, po, fsend, fx, lhs_m, lhs_a,
    w_sem, n_ss, n_rs, e_ss, e_rs, p_ss, p_rs, q_ss, q_rs, a_ss, a_rs, b_ss, b_rs, c_ss, c_rs,
    u_ss, u_rs, d_ss, d_rs, o_ss, o_rs, f_ss, f_rs,
):
    z = lax.axis_index("sp_0")
    x = lax.axis_index("sp_1")
    c = lax.axis_index("sp_2")
    y = lax.axis_index("tp")
    nr = nx * 2
    me = x * 2 + c

    def at_y(d):
        return {"tp": lax.rem(y + d, ny)}

    def at_row(d):
        j = lax.rem(me + d, nr)
        return {"sp_1": j // 2, "sp_2": lax.rem(j, 2)}

    def at_z(d):
        return {"sp_0": lax.rem(z + d, nz)}

    pairs = ((hqd, qd), (hld, ld), (hrt, rt), (hlup, lup), (hqt, qt), (hmq, mq), (hmk, mk), (hmv, mv),
             (hgt, gt), (hmo, mo), (hwm, wm), (hwa, wa))
    loads = [pltpu.make_async_copy(a, b, w_sem.at[i]) for i, (a, b) in enumerate(pairs)]
    for load in loads:
        load.start()
    barrier = pltpu.get_barrier_semaphore()
    peers = [at_y(d) for d in range(1, ny)] + [at_row(d) for d in range(1, nr)] + [at_z(d) for d in range(1, nz)]
    for peer in peers:
        pl.semaphore_signal(barrier, inc=1, device_id=peer, device_id_type=MESH)

    xt = tok[...].astype(F32)
    normed_local = (rms(xt) * gain[...]).astype(BF)
    normed[pl.ds(y, 1)] = normed_local[None]

    segment = (z * nx + x) * 2 + c
    places = (segment * BLOCK + lax.broadcasted_iota(jnp.int32, (16, BLOCK), 1)).astype(F32)
    line = lax.broadcasted_iota(jnp.int32, (16, BLOCK), 0)
    frequency = jnp.zeros((16, BLOCK), F32)
    for j in range(16):
        frequency = jnp.where(line == j, FREQUENCIES[j], frequency)
    angles = places * frequency
    trig[0] = jnp.transpose(jnp.concatenate([jnp.cos(angles)] * 8, axis=0))
    trig[1] = jnp.transpose(jnp.concatenate([jnp.sin(angles)] * 8, axis=0))

    src = lax.broadcasted_iota(jnp.int32, (96, 128), 0)
    dst = lax.broadcasted_iota(jnp.int32, (96, 128), 1)
    rope_own, rope_swap = 64 + lax.rem(dst, 32), 64 + lax.rem(dst + 16, 32)
    q8 = jnp.broadcast_to(qgain[...], (8, 96))
    k8 = jnp.broadcast_to(kgain[...], (8, 96))
    scale = (NOPE + ROPE) ** (-0.5)
    q_own = dot(q8, (src == dst).astype(F32), HI)[0:1] * scale
    q_swap = dot(q8, (src == rope_swap).astype(F32), HI)[0:1] * scale
    k_own = dot(k8, (src == rope_own).astype(F32), HI)[0:1]
    k_swap = dot(k8, (src == rope_swap).astype(F32), HI)[0:1]
    k_plain = dot(k8, (src == dst).astype(F32), HI)[0:1]
    lane1 = lanes((1, 128))
    sign = jnp.where(lax.rem(lane1, 32) < 16, -1.0, 1.0)
    in_rope = jnp.logical_and(lane1 >= 64, lane1 < 96)

    loads[0].wait()
    loads[1].wait()
    qdg_row = jnp.concatenate([qdg[i : i + 1, :] for i in range(3)], axis=1)
    ql = (rms(dot(normed_local, qd[...])) * qdg_row).astype(BF)
    la = (rms(dot(normed_local, ld[...])) * lg[...]).astype(BF)
    loads[2].wait()
    for i in range(4):
        rt4[pl.ds(32 * i, 32), :] = rt[...]
        rt4[pl.ds(128 + 32 * i, 16), :] = rt[pl.ds(16, 16), :]
        rt4[pl.ds(128 + 32 * i + 16, 16), :] = rt[pl.ds(0, 16), :]
    ro = dot_nt(normed_local, rt4[...])
    ra, rb = ro[:, :128], ro[:, 128:]
    rscale = lax.rsqrt(jnp.mean(ra * ra, axis=-1, keepdims=True) + EPSILON)
    lane = lanes((ROWS, 128))
    own_rows = pl.ds(pl.multiple_of(y * ROWS, ROWS), ROWS)
    rot = (ra * rscale) * (trig[0, own_rows, :] * k_own) + (rb * rscale) * (trig[1, own_rows, :] * (k_swap * sign))
    rot = jnp.where(lane // ROPE == y, rot, 0.0).astype(BF)
    ebuf[pl.ds(y, 1), :, 0:256] = la[None]
    ebuf[pl.ds(y, 1), :, 256:384] = rot[None]
    ebuf[pl.ds(y, 1), :, 384:768] = ql[None]

    pl.semaphore_wait(barrier, len(peers))

    def spread_y(buf, ss, rs):
        lo, hi = pl.ds(0, ROWS // 2), pl.ds(ROWS // 2, ROWS // 2)
        below, above = lax.rem(y + ny - 1, ny), lax.rem(y + 1, ny)

        def one(i, slot, part, d):
            return rcopy(buf.at[slot, part], buf.at[slot, part], ss.at[i], rs.at[i], at_y(d))

        direct = [one(0, y, lo, 1), one(3, y, hi, ny - 1), one(1, y, hi, 1), one(4, y, lo, ny - 1)]
        onward = [one(2, below, lo, 1), one(5, above, hi, ny - 1)]
        return direct, onward

    e_direct, e_onward = spread_y(ebuf, e_ss, e_rs)
    n_direct, n_onward = spread_y(normed, n_ss, n_rs)
    for copy in e_direct:
        copy.start()
    loads[3].wait()
    lupf[...] = lup[...].astype(F32)
    loads[4].wait()
    for h in range(2):
        base = 96 * (2 * y + h)
        wqt[h, pl.ds(0, 96), :] = qt[pl.ds(pl.multiple_of(base, 32), 96), :]
        wqt[h, pl.ds(96, 16), :] = qt[pl.ds(pl.multiple_of(base + 80, 16), 16), :]
        wqt[h, pl.ds(112, 16), :] = qt[pl.ds(pl.multiple_of(base + 64, 16), 16), :]
    for i in range(2):
        e_direct[i].wait_recv()
        e_onward[i].start()
    for copy in n_direct:
        copy.start()
    e_direct[2].wait_recv()
    e_direct[3].wait_recv()
    for copy in e_onward:
        copy.wait_recv()

    lane2 = lanes((BLOCK, 128))
    low = lane2 < 64
    la_all = ebuf[:, :, 0:256].reshape(BLOCK, KVR)
    kv = []
    for h in range(2):
        w = lupf[pl.ds(2 * y + h, KVR, stride=8), :].astype(BF)
        t = dot(la_all, w)
        mp = jnp.sum(jnp.where(low, t * t, 0.0), axis=-1, keepdims=True) * (1.0 / NOPE)
        kv.append((t * jnp.where(low, lax.rsqrt(mp + EPSILON) * k_plain, 1.0)).astype(BF))
    rsum = (
        (ebuf[0, :, 256:384].astype(F32) + ebuf[1, :, 256:384].astype(F32))
        + (ebuf[2, :, 256:384].astype(F32) + ebuf[3, :, 256:384].astype(F32))
    ).astype(BF)
    first = c == 0
    kvg[pl.ds(z, 1), 0, pl.ds(0, BLOCK), :] = jnp.where(first, kv[0], kv[1])[None]
    kvg[pl.ds(z, 1), 0, pl.ds(BLOCK, ROWS), :] = rsum[None]
    psend[pl.ds(0, BLOCK), :] = jnp.where(first, kv[1], kv[0])
    psend[pl.ds(BLOCK, ROWS), :] = rsum
    p_copy = rcopy(psend, kvg.at[z, 1], p_ss, p_rs, {"sp_2": 1 - c})
    p_copy.start()

    up, down = {}, {}
    far = nz // 2

    def ring_send(s, r):
        if s < far or r == 0:
            k = lax.rem(z - (s - 1) + nz, nz)
            up[s, r] = rcopy(kvg.at[k, r], kvg.at[k, r], u_ss.at[s, r], u_rs.at[s, r], at_z(1))
            up[s, r].start()
        if s < far or r == 1:
            k = lax.rem(z + (s - 1), nz)
            down[s, r] = rcopy(kvg.at[k, r], kvg.at[k, r], d_ss.at[s, r], d_rs.at[s, r], at_z(nz - 1))
            down[s, r].start()

    def ring_recv(s, r):
        for way in (up, down):
            if (s, r) in way:
                way[s, r].wait_recv()
        if s < far:
            ring_send(s + 1, r)

    ring_send(1, 0)
    ql_all = ebuf[:, :, 384:768].reshape(BLOCK, QR)
    cos_q = trig[0] * jnp.where(in_rope, q_own, 0.0) + jnp.where(lane1 < 64, q_own, 0.0)
    sin_q = trig[1] * jnp.where(in_rope, q_swap * sign, 0.0)
    for h in range(2):
        q = dot_nt(ql_all, wqt[h])
        q2 = q * q
        mp = jnp.sum(jnp.where(low, q2, 0.0), axis=-1, keepdims=True) * (1.0 / NOPE)
        mr = jnp.sum(jnp.where(lane2 >= 96, q2, 0.0), axis=-1, keepdims=True) * (1.0 / ROPE)
        qn = q * jnp.where(low, lax.rsqrt(mp + EPSILON), lax.rsqrt(mr + EPSILON))
        qsend[h] = (qn * cos_q + pltpu.roll(qn, 96, 1) * sin_q).astype(BF)
    q_copies = []
    for d in range(1, nr):
        j = lax.rem(me + d, nr)
        copy = rcopy(qsend.at[lax.rem(j, 2)], qg.at[me], q_ss.at[d], q_rs.at[d], at_row(d))
        copy.start()
        q_copies.append(copy)
    qg[pl.ds(me, 1)] = qsend[pl.ds(c, 1)]
    for i in range(2):
        n_direct[i].wait_recv()
        n_onward[i].start()
    p_copy.wait_recv()
    ring_send(1, 1)

    def fill(slot, d):
        k = lax.rem(z + d + nz, nz)
        for r in range(2):
            base = slot * 512 + r * 256
            kvs = kvg[k, r, pl.ds(0, BLOCK), :]
            kop[pl.ds(base, BLOCK), 0:128] = kvs
            vt[:, base : base + BLOCK] = jnp.transpose(jnp.where(low, jnp.ones_like(kvs), kvs))
            rr = kvg[k, r, pl.ds(BLOCK, ROWS), :]
            for j in range(4):
                kop[pl.ds(base + 64 * j, ROWS), 128:256] = jnp.where(lane // ROPE == j, rr, jnp.zeros_like(rr))

    fill(0, 0)
    n_direct[2].wait_recv()
    n_direct[3].wait_recv()
    for copy in n_onward:
        copy.wait_recv()
    for i in range(5, 9):
        loads[i].wait()
    rows = normed[...].reshape(BLOCK, D)
    mem_q = dot(rows, mq[...]).astype(BF)
    mem_k = (dot(rows, mk[...]) * 0.125).astype(BF)
    mem_v = dot(rows, mv[...]).astype(BF)
    gate_t = dot_nt(gt[...], rows).astype(BF)
    ring_recv(1, 0)

    row8 = lax.broadcasted_iota(jnp.int32, (8, 32), 0)
    col8 = lax.broadcasted_iota(jnp.int32, (8, 32), 1)
    pick = (col8 == (row8 // 2) * 8 + y * 2 + lax.rem(row8, 2)).astype(BF)
    pre = dot(pick, gate_t) + jnp.concatenate([goff[i] for i in range(4)], axis=0)
    low_t = lax.broadcasted_iota(jnp.int32, (128, BLOCK), 0) < 64

    def spread(r0, r1):
        wide = jnp.where(low_t, jnp.broadcast_to(r0, (128, BLOCK)), jnp.broadcast_to(r1, (128, BLOCK)))
        return jnp.transpose(wide)

    log_f = jnp.minimum(pre, 0.0) - jnp.log1p(jnp.exp(-jnp.abs(pre)))
    ti = lax.broadcasted_iota(jnp.int32, (BLOCK, BLOCK), 0)
    si = lax.broadcasted_iota(jnp.int32, (BLOCK, BLOCK), 1)
    masks = (si <= ti, si >= ti)
    zero = jnp.zeros_like(mem_q)
    s_heads = (dot_nt(jnp.where(low, mem_q, zero), mem_k), dot_nt(jnp.where(low, zero, mem_q), mem_k))
    v_f = mem_v.astype(F32)
    k_f = mem_k.astype(F32)
    q_f = mem_q.astype(F32)
    parts = []
    for way in range(2):
        i_wide = spread(pre[4 * way : 4 * way + 1], pre[4 * way + 1 : 4 * way + 2])
        f_wide = spread(log_f[4 * way + 2 : 4 * way + 3], log_f[4 * way + 3 : 4 * way + 4])
        cum = dot(masks[way].astype(F32), f_wide, HI)
        g = i_wide - cum
        g_t = jnp.transpose(g)
        total = jnp.sum(f_wide, axis=0, keepdims=True)
        growth = total + g
        level = jnp.max(growth, axis=0, keepdims=True)
        inflow = jnp.exp(growth - level)
        mat = lax.dot_general(
            inflow * v_f, k_f, (((0,), (0,)), ((), ())), precision=HI, preferred_element_type=F32
        )
        fold = jnp.where(lanes((64, 128)) < 64, mat[:64], mat[64:])
        normal = jnp.sum(inflow * k_f, axis=0, keepdims=True)
        vecs = jnp.concatenate([normal, level, total, jnp.zeros((5, 128), F32)], axis=0)
        for j in range(nr):
            asend[j, way, pl.ds(0, 8), :] = fold[8 * j : 8 * j + 8]
            asend[j, way, pl.ds(8, 8), :] = vecs
        parts.append((cum, g_t))
    a_copies = [
        rcopy(asend.at[lax.rem(me + d, nr)], agot.at[me], a_ss.at[d], a_rs.at[d], at_row(d)) for d in range(1, nr)
    ]
    for copy in a_copies:
        copy.start()
    agot[pl.ds(me, 1)] = asend[pl.ds(me, 1)]
    ring_recv(1, 1)
    own_parts = []
    for way in range(2):
        cum, g_t = parts[way]
        nums, dens, tops = [], [], []
        for h in range(2):
            decay = cum[:, 64 * h : 64 * h + 1] + g_t[64 * h : 64 * h + 1, :]
            decay = jnp.where(masks[way], decay, -jnp.inf)
            top = jnp.max(decay, axis=-1, keepdims=True)
            w = s_heads[h] * jnp.exp(decay - top)
            dens.append(jnp.sum(w, axis=-1, keepdims=True))
            nums.append(dot(w.astype(BF), mem_v))
            tops.append(top)
        own_parts.append((
            jnp.where(low, nums[0], nums[1]), jnp.where(low, dens[0], dens[1]), jnp.where(low, tops[0], tops[1]), cum
        ))
    loads[9].wait()
    out_gate = jax.nn.sigmoid(dot(rows, mo[...]).astype(BF).astype(F32))
    fill(1, -1)
    fill(2, 1)

    def chain(early, late):
        joined = jnp.maximum(late[10:11] + early[1], late[9:10])
        scale_e = jnp.exp(late[10:11] + early[1] - joined)
        scale_l = jnp.exp(late[9:10] - joined)
        return (scale_e * early[0] + scale_l * late, joined, early[2] + late[10:11])

    blank = (jnp.zeros((16, 128), F32), jnp.full((1, 128), FLOOR_LOG, F32), jnp.zeros((1, 128), F32))

    def packed(state):
        mat, level, total = state
        line = lax.broadcasted_iota(jnp.int32, (16, 128), 0)
        return jnp.where(line == 9, level, jnp.where(line == 10, total, mat))

    row_orders = (list(range(nr)), list(reversed(range(nr))))
    z_orders = (list(range(nz)), list(reversed(range(nz))))

    for copy in a_copies:
        copy.wait_recv()
    for way in range(2):
        state = blank
        for j in row_orders[way]:
            state = chain(state, agot[j, way])
        rtot[way] = packed(state)
    b_copies = []
    for d in range(1, nz):
        copy = rcopy(rtot.at[(z + d) // nz], pb.at[z], b_ss.at[d], b_rs.at[d], at_z(d))
        copy.start()
        b_copies.append(copy)
    pb[pl.ds(z, 1)] = jnp.zeros((1, 16, 128), F32)

    for copy in q_copies:
        copy.wait_recv()
    tile_r = lax.broadcasted_iota(jnp.int32, (128, 128), 0)
    tile_c = lax.broadcasted_iota(jnp.int32, (128, 128), 1)
    tile_m = (tile_r == 64 + lax.rem(tile_c, 32)).astype(BF)
    for j in range(nr):
        slab = qg[j]
        qop[j, :, 0:128] = jnp.where(low, slab, jnp.zeros_like(slab))
        qop[j, :, 128:256] = dot(slab, tile_m).astype(BF)

    def attend(begin, end, slots, start):
        def block(i, carry):
            j = lax.rem(me + i + 1, nr)
            qv = qop[j]
            if start:
                top = jnp.full((1, BLOCK), FLOOR_LOG, F32)
                acc = jnp.zeros((128, BLOCK), F32)
            else:
                top = top_s[j, 0:1, :]
                acc = acc_s[j]
            for k in slots:
                s = dot_nt(kop[pl.ds(k * 512, 512), :], qv)
                new = jnp.maximum(top, jnp.max(s, axis=0, keepdims=True))
                p = jnp.exp(s - new).astype(BF)
                acc = acc * jnp.exp(top - new) + dot(vt[:, k * 512 : k * 512 + 512], p)
                top = new
            return finish(i, j, top, acc)

        def keep(i, j, top, acc):
            top_s[j] = jnp.broadcast_to(top, (8, BLOCK))
            acc_s[j] = acc
            return 0

        def send(i, j, top, acc):
            d = lax.rem(i + 1, nr)
            den = acc[0:1, :]
            lse = top + jnp.log(den)
            hi = lse.astype(BF).astype(F32)
            mid = (lse - hi).astype(BF).astype(F32)
            lo = (lse - hi) - mid
            at = lax.broadcasted_iota(jnp.int32, (128, BLOCK), 0)
            msg = jnp.where(at == 0, hi, jnp.where(at == 1, mid, jnp.where(at == 2, lo, acc / den)))
            osend[pl.ds(d, 1)] = jnp.transpose(msg).astype(BF)[None]

            @pl.when(i < nr - 1)
            def _():
                rcopy(osend.at[d], po.at[me], o_ss.at[d], o_rs.at[d], at_row(d)).start()

            return 0

        finish = send if end is None else keep
        stop = nr if end is None else end
        lax.fori_loop(begin, stop, block, 0)

    attend(0, nr // 2, (0, 1, 2), True)
    ring_recv(2, 0)
    attend(nr // 2, nr, (0, 1, 2), True)
    ring_recv(2, 1)
    for copy in b_copies:
        copy.wait_recv()
    for way in range(2):
        state = blank
        for j in z_orders[way]:
            ok = (j < z) if way == 0 else (j > z)
            new = chain(state, pb[j])
            state = tuple(jnp.where(ok, a, b) for a, b in zip(new, state))
        for j in row_orders[way]:
            csend[j, way] = packed(state)
            state = chain(state, agot[j, way])
    c_copies = [
        rcopy(csend.at[lax.rem(me + d, nr)], cgot.at[me], c_ss.at[d], c_rs.at[d], at_row(d)) for d in range(1, nr)
    ]
    for copy in c_copies:
        copy.start()
    cgot[pl.ds(me, 1)] = csend[pl.ds(me, 1)]
    fill(3, -2)
    fill(4, 2)
    attend(0, nr // 2, (3, 4), False)
    ring_recv(3, 0)
    attend(nr // 2, nr, (3, 4), False)
    ring_recv(3, 1)
    for copy in c_copies:
        copy.wait_recv()

    hsum = jnp.zeros((BLOCK, 128), F32)
    bi = lax.broadcasted_iota(jnp.int32, (128, 128), 0) // 64
    bj = lax.broadcasted_iota(jnp.int32, (128, 128), 1) // 64
    ones_block = (bi == bj).astype(F32)
    low64 = lanes((64, 128)) < 64
    for way in range(2):
        fold = jnp.concatenate([cgot[j, way, pl.ds(0, 8), :] for j in range(nr)], axis=0)
        normal = cgot[0, way, pl.ds(8, 1), :]
        level = cgot[0, way, pl.ds(9, 1), :]
        full = jnp.concatenate([jnp.where(low64, fold, 0.0), jnp.where(low64, 0.0, fold)], axis=0)
        num, den, top, cum = own_parts[way]
        carried_log = cum + level
        joined = jnp.maximum(top, carried_log)
        own = jnp.exp(top - joined)
        carried = jnp.exp(carried_log - joined)
        num = num * own + carried * dot_nt(q_f, full, HI)
        den = den * own + carried * dot(q_f * normal, ones_block, HI)
        hsum = hsum + num / jnp.maximum(jnp.abs(den), jnp.exp(-joined))
    mean = dot(hsum * hsum, ones_block, HI) * (1.0 / 64)
    combined = hsum * lax.rsqrt(mean + EPSILON) * mng[pl.ds(y, 1), :]
    mem_rows = (combined * out_gate).astype(BF)
    for j in range(ny):
        fsend[0, j] = mem_rows[64 * j : 64 * j + 64]

    def to_owner(i):
        copies = [
            rcopy(fsend.at[i, lax.rem(y + d, ny)], fx.at[i, y], f_ss.at[i, d], f_rs.at[i, d], at_y(d))
            for d in range(1, ny)
        ]
        for copy in copies:
            copy.start()
        fx[i, pl.ds(y, 1)] = fsend[i, pl.ds(y, 1)]
        return copies

    fm_copies = to_owner(0)
    ring_recv(far, 0)
    ring_recv(far, 1)
    fill(5, -3)
    fill(6, 3)
    fill(7, far)
    attend(0, None, (5, 6, 7), False)
    po[pl.ds(me, 1)] = osend[pl.ds(0, 1)]
    loads[10].wait()
    for copy in fm_copies:
        copy.wait_recv()
    for j in range(ny):
        lhs_m[:, 128 * j : 128 * j + 128] = fx[0, j]
    mixed = dot(lhs_m[...], wm[...])
    o_copies = [rcopy(osend.at[d], po.at[me], o_ss.at[d], o_rs.at[d], at_row(d)) for d in range(1, nr)]
    for copy in o_copies:
        copy.wait_recv()
    heads = []
    for h in range(2):
        msgs = [po[2 * j + h].astype(F32) for j in range(nx)]
        lses = [(m[:, 0:1] + m[:, 1:2]) + m[:, 2:3] for m in msgs]
        joined = functools.reduce(jnp.maximum, lses)
        ws = [jnp.exp(v - joined) for v in lses]
        heads.append(sum(w * m for w, m in zip(ws, msgs)) / sum(ws))
    att = jnp.where(low, pltpu.roll(heads[0], 64, 1), heads[1]).astype(BF)
    for j in range(ny):
        fsend[1, j] = att[64 * j : 64 * j + 64]
    fa_copies = to_owner(1)
    loads[11].wait()
    for copy in fa_copies:
        copy.wait_recv()
    for j in range(ny):
        lhs_a[:, 128 * j : 128 * j + 128] = fx[1, j]
    out[...] = (mixed + dot(lhs_a[...], wa[...])).astype(BF)

    for copies in (e_direct, e_onward, n_direct, n_onward, [p_copy], q_copies, a_copies, b_copies, c_copies,
                   o_copies, fm_copies, fa_copies):
        for copy in copies:
            copy.wait_send()
    for copy in list(up.values()) + list(down.values()):
        copy.wait_send()


def body(nz, nx, ny, tokens, input_gain, memory_query, memory_key, memory_value, memory_outgate, memory_gates,
         gate_offset, memory_norm_gain, query_down, query_down_gain, latent_down, latent_gain, rotary_down,
         query_up, latent_up, query_gain, key_gain, memory_output, attention_output):
    args = (
        tokens, input_gain.reshape(1, D), memory_query, memory_key, memory_value, memory_outgate,
        jnp.transpose(memory_gates, (1, 2, 0)).reshape(32, D),
        jnp.transpose(gate_offset, (0, 2, 1)),
        memory_norm_gain.reshape(4, 128), query_down, query_down_gain.reshape(3, 128), latent_down,
        latent_gain.reshape(1, KVR), rotary_down.T,
        jnp.transpose(query_up, (1, 2, 0)).reshape(8 * (NOPE + ROPE), QR),
        latent_up.reshape(KVR * 8, 128), query_gain.reshape(1, 96), key_gain.reshape(1, 96),
        memory_output, attention_output,
    )
    nr = nx * 2
    in_hbm = {2, 3, 4, 5, 6, 9, 11, 13, 14, 15, 18, 19}
    vmem = pl.BlockSpec(memory_space=pltpu.VMEM)
    hbm = pl.BlockSpec(memory_space=pl.ANY)
    dma = pltpu.SemaphoreType.DMA
    keys = nz * 512
    far = nz // 2 + 1
    scratch = [
        pltpu.VMEM((D, 128), BF), pltpu.VMEM((D, 128), BF), pltpu.VMEM((D, 128), BF), pltpu.VMEM((D, 128), BF),
        pltpu.VMEM((32, D), BF), pltpu.VMEM((D, QR), BF), pltpu.VMEM((D, KVR), BF), pltpu.VMEM((32, D), BF),
        pltpu.VMEM((768, QR), BF), pltpu.VMEM((KVR * 8, 128), BF), pltpu.VMEM((512, D), BF), pltpu.VMEM((512, D), BF),
        pltpu.VMEM((256, D), BF), pltpu.VMEM((2, 128, QR), BF), pltpu.VMEM((KVR * 8, 128), F32),
        pltpu.VMEM((2, BLOCK, 128), F32),
        pltpu.VMEM((ny, ROWS, D), BF), pltpu.VMEM((ny, ROWS, 768), BF),
        pltpu.VMEM((nz, 2, BLOCK + ROWS, 128), BF), pltpu.VMEM((BLOCK + ROWS, 128), BF),
        pltpu.VMEM((2, BLOCK, 128), BF), pltpu.VMEM((nr, BLOCK, 128), BF),
        pltpu.VMEM((nr, 2, 16, 128), F32), pltpu.VMEM((nr, 2, 16, 128), F32), pltpu.VMEM((2, 16, 128), F32),
        pltpu.VMEM((nz, 16, 128), F32), pltpu.VMEM((nr, 2, 16, 128), F32), pltpu.VMEM((nr, 2, 16, 128), F32),
        pltpu.VMEM((nr, BLOCK, 256), BF), pltpu.VMEM((keys, 256), BF), pltpu.VMEM((128, keys), BF),
        pltpu.VMEM((nr, 128, BLOCK), F32), pltpu.VMEM((nr, 8, BLOCK), F32),
        pltpu.VMEM((nr, BLOCK, 128), BF), pltpu.VMEM((nr, BLOCK, 128), BF),
        pltpu.VMEM((2, ny, ROWS, 128), BF), pltpu.VMEM((2, ny, ROWS, 128), BF),
        pltpu.VMEM((ROWS, 512), BF), pltpu.VMEM((ROWS, 512), BF),
        dma((12,)), dma((6,)), dma((6,)), dma((6,)), dma((6,)), dma, dma,
        dma((nr,)), dma((nr,)), dma((nr,)), dma((nr,)), dma((nz,)), dma((nz,)), dma((nr,)), dma((nr,)),
        dma((far, 2)), dma((far, 2)), dma((far, 2)), dma((far, 2)),
        dma((nr,)), dma((nr,)), dma((2, ny)), dma((2, ny)),
    ]
    return pl.pallas_call(
        functools.partial(kernel, nz, nx, ny),
        out_shape=jax.ShapeDtypeStruct((ROWS, D), BF),
        in_specs=[hbm if i in in_hbm else vmem for i in range(len(args))],
        out_specs=vmem,
        scratch_shapes=scratch,
        compiler_params=pltpu.CompilerParams(
            collective_id=0, has_side_effects=True, vmem_limit_bytes=60 * 1024 * 1024
        ),
        name="mixer",
    )(*args)


def solution(mesh):
    ny = mesh.shape["tp"]
    nz, nx = 8, 4
    split = Mesh(mesh.devices.reshape(nz, nx, 2, ny), ("sp_0", "sp_1", "sp_2", "tp"))
    rep = P()
    head = P(None, "tp")
    in_specs = (
        P(SP_TP, None), rep, head, head, head, head, rep, P(None, SP, "tp"),
        rep, rep, rep, rep, rep, rep, rep, rep, rep, rep, rep, rep,
    )
    return jax.shard_map(
        functools.partial(body, nz, nx, ny), mesh=split, in_specs=in_specs, out_specs=P(SP_TP, None), check_vma=False
    )
```

time: 101 us -> 77.2 us (0.76)
  Pallas kernels: 86.4 us -> 74 us
  local copies, waits for them, and re-layouts: 11.6 us -> 1.67 us
    pallas_call x1, Pallas kernels: 86.4 us -> 74 us  [body(): pl.pallas_call(functools.partial(kernel, nz, nx, ny), out_shape=jax.Shape...]
    gather x5 -> x0, local copies, waits for them, and re-layouts: 7.07 us -> none  [the longest x1 1.8 us: tables(): kg = key_gain[jnp.minimum(lane, 63)]]
    reshape x2 -> x0, local copies, waits for them, and re-layouts: 1.98 us -> none  [the longest x1 1.37 us: body(): query_down_gain.reshape(1, QR)]
    unnamed x10 -> x1, local copies, waits for them, and re-layouts: 2.58 us -> 1.67 us
where the time goes in v2:
time: 77.2 us; the launch traced here: 75.6 us
  Pallas kernels  74 us (96%)
  local copies, waits for them, and re-layouts  1.67 us (2%)
    pallas_call x1, Pallas kernels, body(): pl.pallas_call(functools.partial(kernel, nz, nx, ny), out_shape=jax.Shape...  74 us
    unnamed x1, local copies, waits for them, and re-layouts  1.67 us

profile of v2, /device:TPU:2, one launch (start us, length us, event | category | flops | bytes accessed | tf_op | source)
XLA Modules:
  0.0 75.6 jit_solution(7736261310655140286)
XLA Ops:
  0.0 74.0 %mixer.1 = bf16[64,2048]{1,0:T(8,128)(2,1)} custom-call(bf16[64,2048]{1,0:T(8,128)(2,1)} %tok.1, f32[1,2048]{1,0:T(1,128)} %bitcast.19, bf16[2048,128]{1,0:T(8,128)(2,1)} %hmq.1, bf16[2048,128]{1,0:T(8,128)(2,1)} %hmk.1, bf16[2048,128]{1,0:T(8,128)(2,1)} %hmv.1, bf16[2048,128]{1,0:T(8,128)(2,1)} %hmo.1, bf16[32,2048]{1,0:T(8,128)(2,1)} %bitcast.17, ...), custom_call_target="tpu_custom_call" | custom-call | tf_op jit(solution)/shard_map/mixer/pallas_call | solution.py:564
  74.0 1.7 %copy.22 = bf16[64,2048]{1,0:T(8,128)(2,1)} copy(bf16[64,2048]{1,0:T(8,128)(2,1)} %mixer.1) | data formatting | bytes 524288

commit v3 on v2

--- a/solution.py
+++ b/solution.py
@@ -56,7 +56,7 @@
     out,
     mq, mk, mv, mo, gt, qd, ld, rt, qt, lup, wm, wa,
     rt4, wqt, lupf, trig, normed, ebuf, kvg, psend, qsend, qg, asend, agot, rtot, pb, csend, cgot,
-    qop, kop, vt, acc_s, top_s, osend, po, fsend, fx, lhs_m, lhs_a,
+    memp, memg, qop, kop, vt, acc_s, top_s, osend, po, fsend, fx, lhs_m, lhs_a,
     w_sem, n_ss, n_rs, e_ss, e_rs, p_ss, p_rs, q_ss, q_rs, a_ss, a_rs, b_ss, b_rs, c_ss, c_rs,
     u_ss, u_rs, d_ss, d_rs, o_ss, o_rs, f_ss, f_rs,
 ):
@@ -154,6 +154,8 @@
     n_direct, n_onward = spread_y(normed, n_ss, n_rs)
     for copy in e_direct:
         copy.start()
+    for copy in n_direct[:2]:
+        copy.start()
     loads[3].wait()
     lupf[...] = lup[...].astype(F32)
     loads[4].wait()
@@ -165,7 +167,7 @@
     for i in range(2):
         e_direct[i].wait_recv()
         e_onward[i].start()
-    for copy in n_direct:
+    for copy in n_direct[2:]:
         copy.start()
     e_direct[2].wait_recv()
     e_direct[3].wait_recv()
@@ -224,16 +226,17 @@
         mr = jnp.sum(jnp.where(lane2 >= 96, q2, 0.0), axis=-1, keepdims=True) * (1.0 / ROPE)
         qn = q * jnp.where(low, lax.rsqrt(mp + EPSILON), lax.rsqrt(mr + EPSILON))
         qsend[h] = (qn * cos_q + pltpu.roll(qn, 96, 1) * sin_q).astype(BF)
-    q_copies = []
-    for d in range(1, nr):
-        j = lax.rem(me + d, nr)
-        copy = rcopy(qsend.at[lax.rem(j, 2)], qg.at[me], q_ss.at[d], q_rs.at[d], at_row(d))
-        copy.start()
-        q_copies.append(copy)
+    def row_copy(src, dst, ss, rs, i, t):
+        device = {"sp_1": lax.rem(x + i + 1, nx), "sp_2": lax.rem(c + t, 2)}
+        return rcopy(src, dst, ss.at[2 * i + t], rs.at[2 * i + t], device)
+
+    q_copies = {}
+    for i in (nx - 1, 0, nx - 2, 1):
+        for t in range(2):
+            if i < nx - 1 or t == 1:
+                q_copies[i, t] = row_copy(qsend.at[lax.rem(c + t, 2)], qg.at[me], q_ss, q_rs, i, t)
+                q_copies[i, t].start()
     qg[pl.ds(me, 1)] = qsend[pl.ds(c, 1)]
-    for i in range(2):
-        n_direct[i].wait_recv()
-        n_onward[i].start()
     p_copy.wait_recv()
     ring_send(1, 1)
 
@@ -243,29 +246,43 @@
             base = slot * 512 + r * 256
             kvs = kvg[k, r, pl.ds(0, BLOCK), :]
             kop[pl.ds(base, BLOCK), 0:128] = kvs
-            vt[:, base : base + BLOCK] = jnp.transpose(jnp.where(low, jnp.ones_like(kvs), kvs))
+            vt[pl.ds(base, BLOCK), :] = jnp.where(low, jnp.ones_like(kvs), kvs)
             rr = kvg[k, r, pl.ds(BLOCK, ROWS), :]
             for j in range(4):
                 kop[pl.ds(base + 64 * j, ROWS), 128:256] = jnp.where(lane // ROPE == j, rr, jnp.zeros_like(rr))
 
     fill(0, 0)
+    for i in range(5, 9):
+        loads[i].wait()
+    loads[9].wait()
+
+    def project(slot):
+        part = normed[slot]
+        at = pl.ds(pl.multiple_of(slot * ROWS, ROWS), ROWS)
+        memp[0, at, :] = dot(part, mq[...]).astype(BF)
+        memp[1, at, :] = (dot(part, mk[...]) * 0.125).astype(BF)
+        memp[2, at, :] = dot(part, mv[...]).astype(BF)
+        memp[3, at, :] = dot(part, mo[...]).astype(BF)
+        memg[at, :] = dot_nt(part, gt[...]).astype(BF)
+
+    for i in range(2):
+        n_direct[i].wait_recv()
+        n_onward[i].start()
+    project(y)
     n_direct[2].wait_recv()
     n_direct[3].wait_recv()
+    project(lax.rem(y + 1, ny))
+    project(lax.rem(y + ny - 1, ny))
+    ring_recv(1, 0)
     for copy in n_onward:
         copy.wait_recv()
-    for i in range(5, 9):
-        loads[i].wait()
-    rows = normed[...].reshape(BLOCK, D)
-    mem_q = dot(rows, mq[...]).astype(BF)
-    mem_k = (dot(rows, mk[...]) * 0.125).astype(BF)
-    mem_v = dot(rows, mv[...]).astype(BF)
-    gate_t = dot_nt(gt[...], rows).astype(BF)
-    ring_recv(1, 0)
-
+    project(lax.rem(y + 2, ny))
+    mem_q, mem_k, mem_v = memp[0], memp[1], memp[2]
+    ring_recv(1, 1)
     row8 = lax.broadcasted_iota(jnp.int32, (8, 32), 0)
     col8 = lax.broadcasted_iota(jnp.int32, (8, 32), 1)
     pick = (col8 == (row8 // 2) * 8 + y * 2 + lax.rem(row8, 2)).astype(BF)
-    pre = dot(pick, gate_t) + jnp.concatenate([goff[i] for i in range(4)], axis=0)
+    pre = dot_nt(pick, memg[...]) + jnp.concatenate([goff[i] for i in range(4)], axis=0)
     low_t = lax.broadcasted_iota(jnp.int32, (128, BLOCK), 0) < 64
 
     def spread(r0, r1):
@@ -308,7 +325,7 @@
     for copy in a_copies:
         copy.start()
     agot[pl.ds(me, 1)] = asend[pl.ds(me, 1)]
-    ring_recv(1, 1)
+    ring_recv(2, 0)
     own_parts = []
     for way in range(2):
         cum, g_t = parts[way]
@@ -324,8 +341,8 @@
         own_parts.append((
             jnp.where(low, nums[0], nums[1]), jnp.where(low, dens[0], dens[1]), jnp.where(low, tops[0], tops[1]), cum
         ))
-    loads[9].wait()
-    out_gate = jax.nn.sigmoid(dot(rows, mo[...]).astype(BF).astype(F32))
+    ring_recv(2, 1)
+    out_gate = jax.nn.sigmoid(memp[3].astype(F32))
     fill(1, -1)
     fill(2, 1)
 
@@ -345,6 +362,73 @@
     row_orders = (list(range(nr)), list(reversed(range(nr))))
     z_orders = (list(range(nz)), list(reversed(range(nz))))
 
+    tile_r = lax.broadcasted_iota(jnp.int32, (128, 128), 0)
+    tile_c = lax.broadcasted_iota(jnp.int32, (128, 128), 1)
+    tile_m = (tile_r == 64 + lax.rem(tile_c, 32)).astype(BF)
+
+    def take_queries(i):
+        xx = lax.rem(x + i + 1, nx)
+        back = (2 * nx - i - 2) % nx
+        for t in range(2):
+            if (back, t) in q_copies:
+                q_copies[back, t].wait_recv()
+        for t in range(2):
+            slab = qg[2 * xx + t]
+            qop[2 * xx + t, :, 0:128] = jnp.where(low, slab, jnp.zeros_like(slab))
+            qop[2 * xx + t, :, 128:256] = dot(slab, tile_m).astype(BF)
+
+    take_queries(nx - 1)
+    take_queries(0)
+
+    def o_copy(i, t):
+        return row_copy(osend.at[2 * i + t], po.at[me], o_ss, o_rs, i, t)
+
+    def attend(begin, end, slots, start=False, last=False):
+        def block(n, carry):
+            i = lax.rem(n + nx - 1, nx) if start else n
+            xx = lax.rem(x + i + 1, nx)
+            cores = [lax.rem(c + t, 2) for t in range(2)]
+            qv = jnp.concatenate([qop[2 * xx + cores[t]] for t in range(2)], axis=0)
+            if start:
+                top = jnp.full((2 * BLOCK, 128), FLOOR_LOG, F32)
+                acc = jnp.zeros((2 * BLOCK, 128), F32)
+            else:
+                top = top_s[i]
+                acc = acc_s[i]
+            score = dot_nt(qv, kop[pl.ds(slots[0] * 512, 512), :])
+            for k in slots:
+                after = dot_nt(qv, kop[pl.ds((k + 1) * 512, 512), :]) if k != slots[-1] else None
+                new = jnp.maximum(top, jnp.max(score, axis=-1, keepdims=True))
+                p = jnp.exp(score - jnp.concatenate([new] * 4, axis=1)).astype(BF)
+                acc = acc * jnp.exp(top - new) + dot(p, vt[pl.ds(k * 512, 512), :])
+                top = new
+                score = after
+            if not last:
+                top_s[i] = top
+                acc_s[i] = acc
+                return carry
+            at = lanes((2 * BLOCK, 128))
+            den = acc[:, 0:1]
+            lse = top + jnp.log(den)
+            hi = lse.astype(BF).astype(F32)
+            mid = (lse - hi).astype(BF).astype(F32)
+            lo = (lse - hi) - mid
+            msg = jnp.where(at == 0, hi, jnp.where(at == 1, mid, jnp.where(at == 2, lo, acc / den))).astype(BF)
+            for t in range(2):
+                d = 2 * i + t
+                osend[pl.ds(d, 1)] = msg[BLOCK * t : BLOCK * t + BLOCK][None]
+
+                @pl.when(jnp.logical_or(i < nx - 1, t == 1))
+                def _():
+                    o_copy(i, t).start()
+
+            return carry
+
+        lax.fori_loop(begin, end, block, 0)
+
+    half = nr // 4
+    attend(0, half, (0, 1, 2), start=True)
+    ring_recv(3, 0)
     for copy in a_copies:
         copy.wait_recv()
     for way in range(2):
@@ -358,65 +442,14 @@
         copy.start()
         b_copies.append(copy)
     pb[pl.ds(z, 1)] = jnp.zeros((1, 16, 128), F32)
-
-    for copy in q_copies:
-        copy.wait_recv()
-    tile_r = lax.broadcasted_iota(jnp.int32, (128, 128), 0)
-    tile_c = lax.broadcasted_iota(jnp.int32, (128, 128), 1)
-    tile_m = (tile_r == 64 + lax.rem(tile_c, 32)).astype(BF)
-    for j in range(nr):
-        slab = qg[j]
-        qop[j, :, 0:128] = jnp.where(low, slab, jnp.zeros_like(slab))
-        qop[j, :, 128:256] = dot(slab, tile_m).astype(BF)
-
-    def attend(begin, end, slots, start):
-        def block(i, carry):
-            j = lax.rem(me + i + 1, nr)
-            qv = qop[j]
-            if start:
-                top = jnp.full((1, BLOCK), FLOOR_LOG, F32)
-                acc = jnp.zeros((128, BLOCK), F32)
-            else:
-                top = top_s[j, 0:1, :]
-                acc = acc_s[j]
-            for k in slots:
-                s = dot_nt(kop[pl.ds(k * 512, 512), :], qv)
-                new = jnp.maximum(top, jnp.max(s, axis=0, keepdims=True))
-                p = jnp.exp(s - new).astype(BF)
-                acc = acc * jnp.exp(top - new) + dot(vt[:, k * 512 : k * 512 + 512], p)
-                top = new
-            return finish(i, j, top, acc)
-
-        def keep(i, j, top, acc):
-            top_s[j] = jnp.broadcast_to(top, (8, BLOCK))
-            acc_s[j] = acc
-            return 0
-
-        def send(i, j, top, acc):
-            d = lax.rem(i + 1, nr)
-            den = acc[0:1, :]
-            lse = top + jnp.log(den)
-            hi = lse.astype(BF).astype(F32)
-            mid = (lse - hi).astype(BF).astype(F32)
-            lo = (lse - hi) - mid
-            at = lax.broadcasted_iota(jnp.int32, (128, BLOCK), 0)
-            msg = jnp.where(at == 0, hi, jnp.where(at == 1, mid, jnp.where(at == 2, lo, acc / den)))
-            osend[pl.ds(d, 1)] = jnp.transpose(msg).astype(BF)[None]
-
-            @pl.when(i < nr - 1)
-            def _():
-                rcopy(osend.at[d], po.at[me], o_ss.at[d], o_rs.at[d], at_row(d)).start()
-
-            return 0
-
-        finish = send if end is None else keep
-        stop = nr if end is None else end
-        lax.fori_loop(begin, stop, block, 0)
-
-    attend(0, nr // 2, (0, 1, 2), True)
-    ring_recv(2, 0)
-    attend(nr // 2, nr, (0, 1, 2), True)
-    ring_recv(2, 1)
+    take_queries(1)
+    take_queries(2)
+    attend(half, 2 * half, (0, 1, 2), start=True)
+    ring_recv(3, 1)
+    fill(3, -2)
+    fill(4, 2)
+    attend(0, half, (3, 4))
+    attend(half, 2 * half, (3, 4))
     for copy in b_copies:
         copy.wait_recv()
     for way in range(2):
@@ -434,15 +467,15 @@
     for copy in c_copies:
         copy.start()
     cgot[pl.ds(me, 1)] = csend[pl.ds(me, 1)]
-    fill(3, -2)
-    fill(4, 2)
-    attend(0, nr // 2, (3, 4), False)
-    ring_recv(3, 0)
-    attend(nr // 2, nr, (3, 4), False)
-    ring_recv(3, 1)
+    fill(5, -3)
+    fill(6, 3)
+    ring_recv(far, 0)
+    ring_recv(far, 1)
+    fill(7, far)
+    attend(0, 2 * half, (5, 6, 7), last=True)
+    po[pl.ds(me, 1)] = osend[pl.ds(nr - 2, 1)]
     for copy in c_copies:
         copy.wait_recv()
-
     hsum = jnp.zeros((BLOCK, 128), F32)
     bi = lax.broadcasted_iota(jnp.int32, (128, 128), 0) // 64
     bj = lax.broadcasted_iota(jnp.int32, (128, 128), 1) // 64
@@ -478,20 +511,7 @@
         return copies
 
     fm_copies = to_owner(0)
-    ring_recv(far, 0)
-    ring_recv(far, 1)
-    fill(5, -3)
-    fill(6, 3)
-    fill(7, far)
-    attend(0, None, (5, 6, 7), False)
-    po[pl.ds(me, 1)] = osend[pl.ds(0, 1)]
-    loads[10].wait()
-    for copy in fm_copies:
-        copy.wait_recv()
-    for j in range(ny):
-        lhs_m[:, 128 * j : 128 * j + 128] = fx[0, j]
-    mixed = dot(lhs_m[...], wm[...])
-    o_copies = [rcopy(osend.at[d], po.at[me], o_ss.at[d], o_rs.at[d], at_row(d)) for d in range(1, nr)]
+    o_copies = [o_copy(i, t) for i in range(nx) for t in range(2) if i < nx - 1 or t == 1]
     for copy in o_copies:
         copy.wait_recv()
     heads = []
@@ -505,6 +525,12 @@
     for j in range(ny):
         fsend[1, j] = att[64 * j : 64 * j + 64]
     fa_copies = to_owner(1)
+    loads[10].wait()
+    for copy in fm_copies:
+        copy.wait_recv()
+    for j in range(ny):
+        lhs_m[:, 128 * j : 128 * j + 128] = fx[0, j]
+    mixed = dot(lhs_m[...], wm[...])
     loads[11].wait()
     for copy in fa_copies:
         copy.wait_recv()
@@ -512,7 +538,7 @@
         lhs_a[:, 128 * j : 128 * j + 128] = fx[1, j]
     out[...] = (mixed + dot(lhs_a[...], wa[...])).astype(BF)
 
-    for copies in (e_direct, e_onward, n_direct, n_onward, [p_copy], q_copies, a_copies, b_copies, c_copies,
+    for copies in (e_direct, e_onward, n_direct, n_onward, [p_copy], q_copies.values(), a_copies, b_copies, c_copies,
                    o_copies, fm_copies, fa_copies):
         for copy in copies:
             copy.wait_send()
@@ -536,7 +562,7 @@
     nr = nx * 2
     in_hbm = {2, 3, 4, 5, 6, 9, 11, 13, 14, 15, 18, 19}
     vmem = pl.BlockSpec(memory_space=pltpu.VMEM)
-    hbm = pl.BlockSpec(memory_space=pl.ANY)
+    hbm = pl.BlockSpec(memory_space=pltpu.HBM)
     dma = pltpu.SemaphoreType.DMA
     keys = nz * 512
     far = nz // 2 + 1
@@ -551,8 +577,9 @@
         pltpu.VMEM((2, BLOCK, 128), BF), pltpu.VMEM((nr, BLOCK, 128), BF),
         pltpu.VMEM((nr, 2, 16, 128), F32), pltpu.VMEM((nr, 2, 16, 128), F32), pltpu.VMEM((2, 16, 128), F32),
         pltpu.VMEM((nz, 16, 128), F32), pltpu.VMEM((nr, 2, 16, 128), F32), pltpu.VMEM((nr, 2, 16, 128), F32),
-        pltpu.VMEM((nr, BLOCK, 256), BF), pltpu.VMEM((keys, 256), BF), pltpu.VMEM((128, keys), BF),
-        pltpu.VMEM((nr, 128, BLOCK), F32), pltpu.VMEM((nr, 8, BLOCK), F32),
+        pltpu.VMEM((4, BLOCK, 128), BF), pltpu.VMEM((BLOCK, 32), BF),
+        pltpu.VMEM((nr, BLOCK, 256), BF), pltpu.VMEM((keys, 256), BF), pltpu.VMEM((keys, 128), BF),
+        pltpu.VMEM((nr // 2, 2 * BLOCK, 128), F32), pltpu.VMEM((nr // 2, 2 * BLOCK, 128), F32),
         pltpu.VMEM((nr, BLOCK, 128), BF), pltpu.VMEM((nr, BLOCK, 128), BF),
         pltpu.VMEM((2, ny, ROWS, 128), BF), pltpu.VMEM((2, ny, ROWS, 128), BF),
         pltpu.VMEM((ROWS, 512), BF), pltpu.VMEM((ROWS, 512), BF),

time: 77.2 us -> 60.2 us (0.78)
  Pallas kernels: 74 us -> 57.3 us
    pallas_call x1, Pallas kernels: 74 us -> 57.3 us  [body(): pl.pallas_call(functools.partial(kernel, nz, nx, ny), out_shape=jax.Shape...]
where the time goes in v3:
time: 60.2 us; the launch traced here: 59 us
  Pallas kernels  57.3 us (95%)
  local copies, waits for them, and re-layouts  1.67 us (3%)
    pallas_call x1, Pallas kernels, body(): pl.pallas_call(functools.partial(kernel, nz, nx, ny), out_shape=jax.Shape...  57.3 us
    unnamed x1, local copies, waits for them, and re-layouts  1.67 us

profile of v3, /device:TPU:2, one launch (start us, length us, event | category | flops | bytes accessed | tf_op | source)
XLA Modules:
  0.0 59.0 jit_solution(8087706246360751053)
XLA Ops:
  0.0 57.3 %mixer.1 = bf16[64,2048]{1,0:T(8,128)(2,1)} custom-call(bf16[64,2048]{1,0:T(8,128)(2,1)} %tok.1, f32[1,2048]{1,0:T(1,128)} %bitcast.19, bf16[2048,128]{1,0:T(8,128)(2,1)} %hmq.1, bf16[2048,128]{1,0:T(8,128)(2,1)} %hmk.1, bf16[2048,128]{1,0:T(8,128)(2,1)} %hmv.1, bf16[2048,128]{1,0:T(8,128)(2,1)} %hmo.1, bf16[32,2048]{1,0:T(8,128)(2,1)} %bitcast.17, ...), custom_call_target="tpu_custom_call" | custom-call | tf_op jit(solution)/shard_map/mixer/pallas_call | solution.py:591
  57.3 1.7 %copy.22 = bf16[64,2048]{1,0:T(8,128)(2,1)} copy(bf16[64,2048]{1,0:T(8,128)(2,1)} %mixer.1) | data formatting | bytes 524288

commit v4 on v3

--- a/solution.py
+++ b/solution.py
@@ -33,6 +33,14 @@
 
 def dot_nt(a, b, precision=None):
     return lax.dot_general(a, b, (((1,), (1,)), ((), ())), precision=precision, preferred_element_type=F32)
+
+
+def pieces(v, n):
+    found = []
+    for _ in range(n):
+        found.append(v.astype(BF))
+        v = v - found[-1].astype(F32)
+    return found
 
 
 def lanes(shape):
@@ -154,8 +162,6 @@
     n_direct, n_onward = spread_y(normed, n_ss, n_rs)
     for copy in e_direct:
         copy.start()
-    for copy in n_direct[:2]:
-        copy.start()
     loads[3].wait()
     lupf[...] = lup[...].astype(F32)
     loads[4].wait()
@@ -167,7 +173,7 @@
     for i in range(2):
         e_direct[i].wait_recv()
         e_onward[i].start()
-    for copy in n_direct[2:]:
+    for copy in n_direct:
         copy.start()
     e_direct[2].wait_recv()
     e_direct[3].wait_recv()
@@ -252,116 +258,6 @@
                 kop[pl.ds(base + 64 * j, ROWS), 128:256] = jnp.where(lane // ROPE == j, rr, jnp.zeros_like(rr))
 
     fill(0, 0)
-    for i in range(5, 9):
-        loads[i].wait()
-    loads[9].wait()
-
-    def project(slot):
-        part = normed[slot]
-        at = pl.ds(pl.multiple_of(slot * ROWS, ROWS), ROWS)
-        memp[0, at, :] = dot(part, mq[...]).astype(BF)
-        memp[1, at, :] = (dot(part, mk[...]) * 0.125).astype(BF)
-        memp[2, at, :] = dot(part, mv[...]).astype(BF)
-        memp[3, at, :] = dot(part, mo[...]).astype(BF)
-        memg[at, :] = dot_nt(part, gt[...]).astype(BF)
-
-    for i in range(2):
-        n_direct[i].wait_recv()
-        n_onward[i].start()
-    project(y)
-    n_direct[2].wait_recv()
-    n_direct[3].wait_recv()
-    project(lax.rem(y + 1, ny))
-    project(lax.rem(y + ny - 1, ny))
-    ring_recv(1, 0)
-    for copy in n_onward:
-        copy.wait_recv()
-    project(lax.rem(y + 2, ny))
-    mem_q, mem_k, mem_v = memp[0], memp[1], memp[2]
-    ring_recv(1, 1)
-    row8 = lax.broadcasted_iota(jnp.int32, (8, 32), 0)
-    col8 = lax.broadcasted_iota(jnp.int32, (8, 32), 1)
-    pick = (col8 == (row8 // 2) * 8 + y * 2 + lax.rem(row8, 2)).astype(BF)
-    pre = dot_nt(pick, memg[...]) + jnp.concatenate([goff[i] for i in range(4)], axis=0)
-    low_t = lax.broadcasted_iota(jnp.int32, (128, BLOCK), 0) < 64
-
-    def spread(r0, r1):
-        wide = jnp.where(low_t, jnp.broadcast_to(r0, (128, BLOCK)), jnp.broadcast_to(r1, (128, BLOCK)))
-        return jnp.transpose(wide)
-
-    log_f = jnp.minimum(pre, 0.0) - jnp.log1p(jnp.exp(-jnp.abs(pre)))
-    ti = lax.broadcasted_iota(jnp.int32, (BLOCK, BLOCK), 0)
-    si = lax.broadcasted_iota(jnp.int32, (BLOCK, BLOCK), 1)
-    masks = (si <= ti, si >= ti)
-    zero = jnp.zeros_like(mem_q)
-    s_heads = (dot_nt(jnp.where(low, mem_q, zero), mem_k), dot_nt(jnp.where(low, zero, mem_q), mem_k))
-    v_f = mem_v.astype(F32)
-    k_f = mem_k.astype(F32)
-    q_f = mem_q.astype(F32)
-    parts = []
-    for way in range(2):
-        i_wide = spread(pre[4 * way : 4 * way + 1], pre[4 * way + 1 : 4 * way + 2])
-        f_wide = spread(log_f[4 * way + 2 : 4 * way + 3], log_f[4 * way + 3 : 4 * way + 4])
-        cum = dot(masks[way].astype(F32), f_wide, HI)
-        g = i_wide - cum
-        g_t = jnp.transpose(g)
-        total = jnp.sum(f_wide, axis=0, keepdims=True)
-        growth = total + g
-        level = jnp.max(growth, axis=0, keepdims=True)
-        inflow = jnp.exp(growth - level)
-        mat = lax.dot_general(
-            inflow * v_f, k_f, (((0,), (0,)), ((), ())), precision=HI, preferred_element_type=F32
-        )
-        fold = jnp.where(lanes((64, 128)) < 64, mat[:64], mat[64:])
-        normal = jnp.sum(inflow * k_f, axis=0, keepdims=True)
-        vecs = jnp.concatenate([normal, level, total, jnp.zeros((5, 128), F32)], axis=0)
-        for j in range(nr):
-            asend[j, way, pl.ds(0, 8), :] = fold[8 * j : 8 * j + 8]
-            asend[j, way, pl.ds(8, 8), :] = vecs
-        parts.append((cum, g_t))
-    a_copies = [
-        rcopy(asend.at[lax.rem(me + d, nr)], agot.at[me], a_ss.at[d], a_rs.at[d], at_row(d)) for d in range(1, nr)
-    ]
-    for copy in a_copies:
-        copy.start()
-    agot[pl.ds(me, 1)] = asend[pl.ds(me, 1)]
-    ring_recv(2, 0)
-    own_parts = []
-    for way in range(2):
-        cum, g_t = parts[way]
-        nums, dens, tops = [], [], []
-        for h in range(2):
-            decay = cum[:, 64 * h : 64 * h + 1] + g_t[64 * h : 64 * h + 1, :]
-            decay = jnp.where(masks[way], decay, -jnp.inf)
-            top = jnp.max(decay, axis=-1, keepdims=True)
-            w = s_heads[h] * jnp.exp(decay - top)
-            dens.append(jnp.sum(w, axis=-1, keepdims=True))
-            nums.append(dot(w.astype(BF), mem_v))
-            tops.append(top)
-        own_parts.append((
-            jnp.where(low, nums[0], nums[1]), jnp.where(low, dens[0], dens[1]), jnp.where(low, tops[0], tops[1]), cum
-        ))
-    ring_recv(2, 1)
-    out_gate = jax.nn.sigmoid(memp[3].astype(F32))
-    fill(1, -1)
-    fill(2, 1)
-
-    def chain(early, late):
-        joined = jnp.maximum(late[10:11] + early[1], late[9:10])
-        scale_e = jnp.exp(late[10:11] + early[1] - joined)
-        scale_l = jnp.exp(late[9:10] - joined)
-        return (scale_e * early[0] + scale_l * late, joined, early[2] + late[10:11])
-
-    blank = (jnp.zeros((16, 128), F32), jnp.full((1, 128), FLOOR_LOG, F32), jnp.zeros((1, 128), F32))
-
-    def packed(state):
-        mat, level, total = state
-        line = lax.broadcasted_iota(jnp.int32, (16, 128), 0)
-        return jnp.where(line == 9, level, jnp.where(line == 10, total, mat))
-
-    row_orders = (list(range(nr)), list(reversed(range(nr))))
-    z_orders = (list(range(nz)), list(reversed(range(nz))))
-
     tile_r = lax.broadcasted_iota(jnp.int32, (128, 128), 0)
     tile_c = lax.broadcasted_iota(jnp.int32, (128, 128), 1)
     tile_m = (tile_r == 64 + lax.rem(tile_c, 32)).astype(BF)
@@ -376,9 +272,6 @@
             slab = qg[2 * xx + t]
             qop[2 * xx + t, :, 0:128] = jnp.where(low, slab, jnp.zeros_like(slab))
             qop[2 * xx + t, :, 128:256] = dot(slab, tile_m).astype(BF)
-
-    take_queries(nx - 1)
-    take_queries(0)
 
     def o_copy(i, t):
         return row_copy(osend.at[2 * i + t], po.at[me], o_ss, o_rs, i, t)
@@ -407,16 +300,18 @@
                 top_s[i] = top
                 acc_s[i] = acc
                 return carry
-            at = lanes((2 * BLOCK, 128))
             den = acc[:, 0:1]
-            lse = top + jnp.log(den)
-            hi = lse.astype(BF).astype(F32)
-            mid = (lse - hi).astype(BF).astype(F32)
-            lo = (lse - hi) - mid
-            msg = jnp.where(at == 0, hi, jnp.where(at == 1, mid, jnp.where(at == 2, lo, acc / den))).astype(BF)
+            lse = top + jnp.log(acc)
+            share = acc / den
+            low1 = lane2[:128] < 64
             for t in range(2):
                 d = 2 * i + t
-                osend[pl.ds(d, 1)] = msg[BLOCK * t : BLOCK * t + BLOCK][None]
+                a0, a1 = share[256 * t : 256 * t + 128], share[256 * t + 128 : 256 * t + 256]
+                l0, l1 = lse[256 * t : 256 * t + 128], lse[256 * t + 128 : 256 * t + 256]
+                osend[d, pl.ds(0, 128), :] = jnp.where(low1, pltpu.roll(a0, 64, 1), a1).astype(BF)
+                rows_l = jnp.transpose(jnp.where(low1, l0, pltpu.roll(l1, 64, 1)))
+                three = pieces(jnp.concatenate([rows_l[0:1], rows_l[64:65]], axis=0), 3)
+                osend[d, pl.ds(128, 16), :] = jnp.concatenate(three + [jnp.zeros((10, 128), BF)], axis=0)
 
                 @pl.when(jnp.logical_or(i < nx - 1, t == 1))
                 def _():
@@ -427,7 +322,134 @@
         lax.fori_loop(begin, end, block, 0)
 
     half = nr // 4
-    attend(0, half, (0, 1, 2), start=True)
+    for i in range(5, 9):
+        loads[i].wait()
+    loads[9].wait()
+
+    def project(slot):
+        part = normed[slot]
+        at = pl.ds(pl.multiple_of(slot * ROWS, ROWS), ROWS)
+        memp[0, at, :] = dot(part, mq[...]).astype(BF)
+        memp[1, at, :] = (dot(part, mk[...]) * 0.125).astype(BF)
+        memp[2, at, :] = dot(part, mv[...]).astype(BF)
+        memp[3, at, :] = dot(part, mo[...]).astype(BF)
+        memg[at, :] = dot_nt(part, gt[...]).astype(BF)
+
+    for i in range(2):
+        n_direct[i].wait_recv()
+        n_onward[i].start()
+    project(y)
+    n_direct[2].wait_recv()
+    n_direct[3].wait_recv()
+    project(lax.rem(y + 1, ny))
+    project(lax.rem(y + ny - 1, ny))
+    ring_recv(1, 0)
+    take_queries(nx - 1)
+    ring_recv(1, 1)
+    fill(1, -1)
+    fill(2, 1)
+    attend(0, 1, (0, 1, 2), start=True)
+    for copy in n_onward:
+        copy.wait_recv()
+    project(lax.rem(y + 2, ny))
+    mem_q, mem_k, mem_v = memp[0], memp[1], memp[2]
+    row8 = lax.broadcasted_iota(jnp.int32, (8, 32), 0)
+    col8 = lax.broadcasted_iota(jnp.int32, (8, 32), 1)
+    pick = (col8 == (row8 // 2) * 8 + y * 2 + lax.rem(row8, 2)).astype(BF)
+    pre = dot_nt(pick, memg[...]) + jnp.concatenate([goff[i] for i in range(4)], axis=0)
+    low_t = lax.broadcasted_iota(jnp.int32, (128, BLOCK), 0) < 64
+
+    def spread(r0, r1):
+        wide = jnp.where(low_t, jnp.broadcast_to(r0, (128, BLOCK)), jnp.broadcast_to(r1, (128, BLOCK)))
+        return jnp.transpose(wide)
+
+    log_f = jnp.minimum(pre, 0.0) - jnp.log1p(jnp.exp(-jnp.abs(pre)))
+    ti = lax.broadcasted_iota(jnp.int32, (BLOCK, BLOCK), 0)
+    si = lax.broadcasted_iota(jnp.int32, (BLOCK, BLOCK), 1)
+    masks = (si <= ti, si >= ti)
+    log_3 = pieces(log_f, 3)
+    zero = jnp.zeros_like(mem_q)
+    v_f = mem_v.astype(F32)
+    parts = []
+    line16 = lax.broadcasted_iota(jnp.int32, (8, 128), 0)
+    lane8 = lanes((8, 128))
+    for way in range(2):
+        ones = masks[1 - way].astype(BF)
+        cums = (dot(log_3[0], ones) + dot(log_3[1], ones)) + dot(log_3[2], ones)
+        cum = cums[4 * way + 2 : 4 * way + 4]
+        g = pre[4 * way : 4 * way + 2] - cum
+        last = BLOCK - 1 if way == 0 else 0
+        total = cum[:, last : last + 1]
+        growth = total + g
+        level = jnp.max(growth, axis=-1, keepdims=True)
+        inflow = jnp.exp(growth - level)
+        wide = spread(inflow[0:1], inflow[1:2])
+        vw = pieces(wide * v_f, 2)
+        mat = sum(
+            lax.dot_general(a, mem_k, (((0,), (0,)), ((), ())), preferred_element_type=F32) for a in vw
+        )
+        fold = jnp.where(lanes((64, 128)) < 64, mat[:64], mat[64:])
+        inflow8 = jnp.concatenate([inflow, jnp.zeros((6, BLOCK), F32)], axis=0)
+        sums = sum(dot(a, mem_k) for a in pieces(inflow8, 2))
+        normal = jnp.where(lane1 < 64, sums[0:1], sums[1:2])
+
+        def by_lane(v):
+            return jnp.where(lane8 < 64, jnp.broadcast_to(v[0:1], (8, 128)), jnp.broadcast_to(v[1:2], (8, 128)))
+
+        vecs = jnp.where(line16 == 0, normal, jnp.where(line16 == 1, by_lane(level), by_lane(total)))
+        for j in range(nr):
+            asend[j, way, pl.ds(0, 8), :] = fold[8 * j : 8 * j + 8]
+            asend[j, way, pl.ds(8, 8), :] = vecs
+        parts.append((cum, g))
+    a_copies = [
+        rcopy(asend.at[lax.rem(me + d, nr)], agot.at[me], a_ss.at[d], a_rs.at[d], at_row(d)) for d in range(1, nr)
+    ]
+    for copy in a_copies:
+        copy.start()
+    agot[pl.ds(me, 1)] = asend[pl.ds(me, 1)]
+    ring_recv(2, 0)
+    own_parts = []
+    s_heads = (dot_nt(jnp.where(low, mem_q, zero), mem_k), dot_nt(jnp.where(low, zero, mem_q), mem_k))
+    for way in range(2):
+        cum, g_t = parts[way]
+        cum = spread(cum[0:1], cum[1:2])
+        nums, dens, tops = [], [], []
+        for h in range(2):
+            decay = cum[:, 64 * h : 64 * h + 1] + g_t[h : h + 1, :]
+            decay = jnp.where(masks[way], decay, -jnp.inf)
+            top = jnp.max(decay, axis=-1, keepdims=True)
+            w = s_heads[h] * jnp.exp(decay - top)
+            dens.append(jnp.sum(w, axis=-1, keepdims=True))
+            nums.append(dot(w.astype(BF), mem_v))
+            tops.append(top)
+        own_parts.append((
+            jnp.where(low, nums[0], nums[1]), jnp.where(low, dens[0], dens[1]), jnp.where(low, tops[0], tops[1]), cum
+        ))
+    ring_recv(2, 1)
+    out_gate = jax.nn.sigmoid(memp[3].astype(F32))
+
+    def chain(early, late):
+        joined = jnp.maximum(late[10:11] + early[1], late[9:10])
+        scale_e = jnp.exp(late[10:11] + early[1] - joined)
+        scale_l = jnp.exp(late[9:10] - joined)
+        return (scale_e * early[0] + scale_l * late, joined, early[2] + late[10:11])
+
+    blank = (jnp.zeros((16, 128), F32), jnp.full((1, 128), FLOOR_LOG, F32), jnp.zeros((1, 128), F32))
+
+    def packed(state):
+        mat, level, total = state
+        line = lax.broadcasted_iota(jnp.int32, (16, 128), 0)
+        return jnp.where(line == 9, level, jnp.where(line == 10, total, mat))
+
+    row_orders = (list(range(nr)), list(reversed(range(nr))))
+    z_orders = (list(range(nz)), list(reversed(range(nz))))
+
+    take_queries(0)
+
+    attend(1, 2, (0, 1, 2), start=True)
+    take_queries(1)
+    take_queries(2)
+    attend(2, 3, (0, 1, 2), start=True)
     ring_recv(3, 0)
     for copy in a_copies:
         copy.wait_recv()
@@ -442,9 +464,7 @@
         copy.start()
         b_copies.append(copy)
     pb[pl.ds(z, 1)] = jnp.zeros((1, 16, 128), F32)
-    take_queries(1)
-    take_queries(2)
-    attend(half, 2 * half, (0, 1, 2), start=True)
+    attend(3, 4, (0, 1, 2), start=True)
     ring_recv(3, 1)
     fill(3, -2)
     fill(4, 2)
@@ -491,10 +511,12 @@
         joined = jnp.maximum(top, carried_log)
         own = jnp.exp(top - joined)
         carried = jnp.exp(carried_log - joined)
-        num = num * own + carried * dot_nt(q_f, full, HI)
-        den = den * own + carried * dot(q_f * normal, ones_block, HI)
+        both = jnp.concatenate([full, ones_block * normal], axis=0)
+        in_q = sum(dot_nt(mem_q, a) for a in pieces(both, 2))
+        num = num * own + carried * in_q[:, :128]
+        den = den * own + carried * in_q[:, 128:]
         hsum = hsum + num / jnp.maximum(jnp.abs(den), jnp.exp(-joined))
-    mean = dot(hsum * hsum, ones_block, HI) * (1.0 / 64)
+    mean = sum(dot(a, ones_block.astype(BF)) for a in pieces(hsum * hsum, 2)) * (1.0 / 64)
     combined = hsum * lax.rsqrt(mean + EPSILON) * mng[pl.ds(y, 1), :]
     mem_rows = (combined * out_gate).astype(BF)
     for j in range(ny):
@@ -515,13 +537,26 @@
     for copy in o_copies:
         copy.wait_recv()
     heads = []
+    low_s = lax.broadcasted_iota(jnp.int32, (128, 128), 0) < 64
+    low1 = lane2[:128] < 64
     for h in range(2):
-        msgs = [po[2 * j + h].astype(F32) for j in range(nx)]
-        lses = [(m[:, 0:1] + m[:, 1:2]) + m[:, 2:3] for m in msgs]
+        lses = []
+        for j in range(nx):
+            st = po[2 * j + h, pl.ds(128, 16), :].astype(F32)
+            lses.append((st[0:2] + st[2:4]) + st[4:6])
         joined = functools.reduce(jnp.maximum, lses)
         ws = [jnp.exp(v - joined) for v in lses]
-        heads.append(sum(w * m for w, m in zip(ws, msgs)) / sum(ws))
-    att = jnp.where(low, pltpu.roll(heads[0], 64, 1), heads[1]).astype(BF)
+        all_w = functools.reduce(jnp.add, ws)
+        out_h = jnp.zeros((128, 128), F32)
+        for j in range(nx):
+            w = ws[j] / all_w
+            wide = jnp.where(low_s, jnp.broadcast_to(w[0:1], (128, 128)), jnp.broadcast_to(w[1:2], (128, 128)))
+            out_h = out_h + jnp.transpose(wide) * po[2 * j + h, pl.ds(0, 128), :].astype(F32)
+        heads.append(out_h)
+    att = jnp.concatenate(
+        [jnp.where(low1, heads[0], pltpu.roll(heads[1], 64, 1)), jnp.where(low1, pltpu.roll(heads[0], 64, 1), heads[1])],
+        axis=0,
+    ).astype(BF)
     for j in range(ny):
         fsend[1, j] = att[64 * j : 64 * j + 64]
     fa_copies = to_owner(1)
@@ -536,7 +571,7 @@
         copy.wait_recv()
     for j in range(ny):
         lhs_a[:, 128 * j : 128 * j + 128] = fx[1, j]
-    out[...] = (mixed + dot(lhs_a[...], wa[...])).astype(BF)
+    out[...] = mixed + dot(lhs_a[...], wa[...])
 
     for copies in (e_direct, e_onward, n_direct, n_onward, [p_copy], q_copies.values(), a_copies, b_copies, c_copies,
                    o_copies, fm_copies, fa_copies):
@@ -580,7 +615,7 @@
         pltpu.VMEM((4, BLOCK, 128), BF), pltpu.VMEM((BLOCK, 32), BF),
         pltpu.VMEM((nr, BLOCK, 256), BF), pltpu.VMEM((keys, 256), BF), pltpu.VMEM((keys, 128), BF),
         pltpu.VMEM((nr // 2, 2 * BLOCK, 128), F32), pltpu.VMEM((nr // 2, 2 * BLOCK, 128), F32),
-        pltpu.VMEM((nr, BLOCK, 128), BF), pltpu.VMEM((nr, BLOCK, 128), BF),
+        pltpu.VMEM((nr, 144, 128), BF), pltpu.VMEM((nr, 144, 128), BF),
         pltpu.VMEM((2, ny, ROWS, 128), BF), pltpu.VMEM((2, ny, ROWS, 128), BF),
         pltpu.VMEM((ROWS, 512), BF), pltpu.VMEM((ROWS, 512), BF),
         dma((12,)), dma((6,)), dma((6,)), dma((6,)), dma((6,)), dma, dma,
@@ -588,9 +623,9 @@
         dma((far, 2)), dma((far, 2)), dma((far, 2)), dma((far, 2)),
         dma((nr,)), dma((nr,)), dma((2, ny)), dma((2, ny)),
     ]
-    return pl.pallas_call(
+    mixed = pl.pallas_call(
         functools.partial(kernel, nz, nx, ny),
-        out_shape=jax.ShapeDtypeStruct((ROWS, D), BF),
+        out_shape=jax.ShapeDtypeStruct((ROWS, D), F32),
         in_specs=[hbm if i in in_hbm else vmem for i in range(len(args))],
         out_specs=vmem,
         scratch_shapes=scratch,
@@ -599,6 +634,7 @@
         ),
         name="mixer",
     )(*args)
+    return mixed.astype(BF)
 
 
 def solution(mesh):

time: 60.2 us -> 56.3 us (0.935); the launches traced: 59 us -> 55.8 us
  Pallas kernels: 57.3 us -> 54 us
  other arithmetic: 0 us -> 1.77 us
  local copies, waits for them, and re-layouts: 1.67 us -> 0 us
    pallas_call x1, Pallas kernels: 57.3 us -> 54 us  [body(): pl.pallas_call(functools.partial(kernel, nz, nx, ny), out_shape=jax.Shape...]
    convert_element_type x0 -> x1, other arithmetic: none -> 1.77 us  [body(): return mixed.astype(BF)]
    unnamed x1 -> x0, local copies, waits for them, and re-layouts: 1.67 us -> none
where the time goes in v4:
time: 56.3 us; the launch traced here: 55.8 us
  Pallas kernels  54 us (96%)
  other arithmetic  1.77 us (3%)
    pallas_call x1, Pallas kernels, body(): pl.pallas_call(functools.partial(kernel, nz, nx, ny), out_shape=jax.Shape...  54 us
    convert_element_type x1, other arithmetic, body(): return mixed.astype(BF)  1.77 us

profile of v4, /device:TPU:2, one launch (start us, length us, event | category | flops | bytes accessed | tf_op | source)
XLA Modules:
  0.0 55.8 jit_solution(8662999901778731766)
XLA Ops:
  0.0 54.0 %mixer.1 = f32[64,2048]{1,0:T(8,128)} custom-call(bf16[64,2048]{1,0:T(8,128)(2,1)} %tok.1, f32[1,2048]{1,0:T(1,128)} %bitcast.19, bf16[2048,128]{1,0:T(8,128)(2,1)} %hmq.1, bf16[2048,128]{1,0:T(8,128)(2,1)} %hmk.1, bf16[2048,128]{1,0:T(8,128)(2,1)} %hmv.1, bf16[2048,128]{1,0:T(8,128)(2,1)} %hmo.1, bf16[32,2048]{1,0:T(8,128)(2,1)} %bitcast.17, ...), custom_call_target="tpu_custom_call" | custom-call | tf_op jit(solution)/shard_map/mixer/pallas_call | solution.py:626
  54.0 1.8 %convert_element_type.3 = bf16[64,2048]{1,0:T(8,128)(2,1)} convert(f32[64,2048]{1,0:T(8,128)} %mixer.1) | non-fusion elementwise | flops 131072 | bytes 786432 | tf_op jit(solution)/shard_map/convert_element_type | solution.py:637

commit v5 on v4

--- a/solution.py
+++ b/solution.py
@@ -63,9 +63,9 @@
     qgain, kgain, hwm, hwa,
     out,
     mq, mk, mv, mo, gt, qd, ld, rt, qt, lup, wm, wa,
-    rt4, wqt, lupf, trig, normed, ebuf, kvg, psend, qsend, qg, asend, agot, rtot, pb, csend, cgot,
+    rt4, wqt, lupf, trig, normed, ebuf, qbuf, kvg, psend, qsend, qg, asend, agot, rtot, pb, csend, cgot,
     memp, memg, qop, kop, vt, acc_s, top_s, osend, po, fsend, fx, lhs_m, lhs_a,
-    w_sem, n_ss, n_rs, e_ss, e_rs, p_ss, p_rs, q_ss, q_rs, a_ss, a_rs, b_ss, b_rs, c_ss, c_rs,
+    w_sem, n_ss, n_rs, e_ss, e_rs, l_ss, l_rs, p_ss, p_rs, q_ss, q_rs, a_ss, a_rs, b_ss, b_rs, c_ss, c_rs,
     u_ss, u_rs, d_ss, d_rs, o_ss, o_rs, f_ss, f_rs,
 ):
     z = lax.axis_index("sp_0")
@@ -85,7 +85,7 @@
     def at_z(d):
         return {"sp_0": lax.rem(z + d, nz)}
 
-    pairs = ((hqd, qd), (hld, ld), (hrt, rt), (hlup, lup), (hqt, qt), (hmq, mq), (hmk, mk), (hmv, mv),
+    pairs = ((hld, ld), (hrt, rt), (hqd, qd), (hlup, lup), (hqt, qt), (hmq, mq), (hmk, mk), (hmv, mv),
              (hgt, gt), (hmo, mo), (hwm, wm), (hwa, wa))
     loads = [pltpu.make_async_copy(a, b, w_sem.at[i]) for i, (a, b) in enumerate(pairs)]
     for load in loads:
@@ -125,11 +125,8 @@
     in_rope = jnp.logical_and(lane1 >= 64, lane1 < 96)
 
     loads[0].wait()
+    la = (rms(dot(normed_local, ld[...])) * lg[...]).astype(BF)
     loads[1].wait()
-    qdg_row = jnp.concatenate([qdg[i : i + 1, :] for i in range(3)], axis=1)
-    ql = (rms(dot(normed_local, qd[...])) * qdg_row).astype(BF)
-    la = (rms(dot(normed_local, ld[...])) * lg[...]).astype(BF)
-    loads[2].wait()
     for i in range(4):
         rt4[pl.ds(32 * i, 32), :] = rt[...]
         rt4[pl.ds(128 + 32 * i, 16), :] = rt[pl.ds(16, 16), :]
@@ -143,7 +140,6 @@
     rot = jnp.where(lane // ROPE == y, rot, 0.0).astype(BF)
     ebuf[pl.ds(y, 1), :, 0:256] = la[None]
     ebuf[pl.ds(y, 1), :, 256:384] = rot[None]
-    ebuf[pl.ds(y, 1), :, 384:768] = ql[None]
 
     pl.semaphore_wait(barrier, len(peers))
 
@@ -159,8 +155,14 @@
         return direct, onward
 
     e_direct, e_onward = spread_y(ebuf, e_ss, e_rs)
+    l_direct, l_onward = spread_y(qbuf, l_ss, l_rs)
     n_direct, n_onward = spread_y(normed, n_ss, n_rs)
     for copy in e_direct:
+        copy.start()
+    loads[2].wait()
+    qdg_row = jnp.concatenate([qdg[i : i + 1, :] for i in range(3)], axis=1)
+    qbuf[pl.ds(y, 1)] = (rms(dot(normed_local, qd[...])) * qdg_row).astype(BF)[None]
+    for copy in l_direct:
         copy.start()
     loads[3].wait()
     lupf[...] = lup[...].astype(F32)
@@ -173,6 +175,9 @@
     for i in range(2):
         e_direct[i].wait_recv()
         e_onward[i].start()
+    for i in range(2):
+        l_direct[i].wait_recv()
+        l_onward[i].start()
     for copy in n_direct:
         copy.start()
     e_direct[2].wait_recv()
@@ -222,7 +227,11 @@
             ring_send(s + 1, r)
 
     ring_send(1, 0)
-    ql_all = ebuf[:, :, 384:768].reshape(BLOCK, QR)
+    l_direct[2].wait_recv()
+    l_direct[3].wait_recv()
+    for copy in l_onward:
+        copy.wait_recv()
+    ql_all = qbuf[...].reshape(BLOCK, QR)
     cos_q = trig[0] * jnp.where(in_rope, q_own, 0.0) + jnp.where(lane1 < 64, q_own, 0.0)
     sin_q = trig[1] * jnp.where(in_rope, q_swap * sign, 0.0)
     for h in range(2):
@@ -408,25 +417,7 @@
         copy.start()
     agot[pl.ds(me, 1)] = asend[pl.ds(me, 1)]
     ring_recv(2, 0)
-    own_parts = []
-    s_heads = (dot_nt(jnp.where(low, mem_q, zero), mem_k), dot_nt(jnp.where(low, zero, mem_q), mem_k))
-    for way in range(2):
-        cum, g_t = parts[way]
-        cum = spread(cum[0:1], cum[1:2])
-        nums, dens, tops = [], [], []
-        for h in range(2):
-            decay = cum[:, 64 * h : 64 * h + 1] + g_t[h : h + 1, :]
-            decay = jnp.where(masks[way], decay, -jnp.inf)
-            top = jnp.max(decay, axis=-1, keepdims=True)
-            w = s_heads[h] * jnp.exp(decay - top)
-            dens.append(jnp.sum(w, axis=-1, keepdims=True))
-            nums.append(dot(w.astype(BF), mem_v))
-            tops.append(top)
-        own_parts.append((
-            jnp.where(low, nums[0], nums[1]), jnp.where(low, dens[0], dens[1]), jnp.where(low, tops[0], tops[1]), cum
-        ))
     ring_recv(2, 1)
-    out_gate = jax.nn.sigmoid(memp[3].astype(F32))
 
     def chain(early, late):
         joined = jnp.maximum(late[10:11] + early[1], late[9:10])
@@ -494,6 +485,24 @@
     fill(7, far)
     attend(0, 2 * half, (5, 6, 7), last=True)
     po[pl.ds(me, 1)] = osend[pl.ds(nr - 2, 1)]
+    own_parts = []
+    s_heads = (dot_nt(jnp.where(low, mem_q, zero), mem_k), dot_nt(jnp.where(low, zero, mem_q), mem_k))
+    for way in range(2):
+        cum, g_t = parts[way]
+        cum = spread(cum[0:1], cum[1:2])
+        nums, dens, tops = [], [], []
+        for h in range(2):
+            decay = cum[:, 64 * h : 64 * h + 1] + g_t[h : h + 1, :]
+            decay = jnp.where(masks[way], decay, -jnp.inf)
+            top = jnp.max(decay, axis=-1, keepdims=True)
+            w = s_heads[h] * jnp.exp(decay - top)
+            dens.append(jnp.sum(w, axis=-1, keepdims=True))
+            nums.append(dot(w.astype(BF), mem_v))
+            tops.append(top)
+        own_parts.append((
+            jnp.where(low, nums[0], nums[1]), jnp.where(low, dens[0], dens[1]), jnp.where(low, tops[0], tops[1]), cum
+        ))
+    out_gate = jax.nn.sigmoid(memp[3].astype(F32))
     for copy in c_copies:
         copy.wait_recv()
     hsum = jnp.zeros((BLOCK, 128), F32)
@@ -571,9 +580,9 @@
         copy.wait_recv()
     for j in range(ny):
         lhs_a[:, 128 * j : 128 * j + 128] = fx[1, j]
-    out[...] = mixed + dot(lhs_a[...], wa[...])
-
-    for copies in (e_direct, e_onward, n_direct, n_onward, [p_copy], q_copies.values(), a_copies, b_copies, c_copies,
+    out[...] = (mixed + dot(lhs_a[...], wa[...])).astype(BF)
+
+    for copies in (e_direct, e_onward, l_direct, l_onward, n_direct, n_onward, [p_copy], q_copies.values(), a_copies, b_copies, c_copies,
                    o_copies, fm_copies, fa_copies):
         for copy in copies:
             copy.wait_send()
@@ -607,7 +616,7 @@
         pltpu.VMEM((768, QR), BF), pltpu.VMEM((KVR * 8, 128), BF), pltpu.VMEM((512, D), BF), pltpu.VMEM((512, D), BF),
         pltpu.VMEM((256, D), BF), pltpu.VMEM((2, 128, QR), BF), pltpu.VMEM((KVR * 8, 128), F32),
         pltpu.VMEM((2, BLOCK, 128), F32),
-        pltpu.VMEM((ny, ROWS, D), BF), pltpu.VMEM((ny, ROWS, 768), BF),
+        pltpu.VMEM((ny, ROWS, D), BF), pltpu.VMEM((ny, ROWS, 384), BF), pltpu.VMEM((ny, ROWS, QR), BF),
         pltpu.VMEM((nz, 2, BLOCK + ROWS, 128), BF), pltpu.VMEM((BLOCK + ROWS, 128), BF),
         pltpu.VMEM((2, BLOCK, 128), BF), pltpu.VMEM((nr, BLOCK, 128), BF),
         pltpu.VMEM((nr, 2, 16, 128), F32), pltpu.VMEM((nr, 2, 16, 128), F32), pltpu.VMEM((2, 16, 128), F32),
@@ -618,14 +627,14 @@
         pltpu.VMEM((nr, 144, 128), BF), pltpu.VMEM((nr, 144, 128), BF),
         pltpu.VMEM((2, ny, ROWS, 128), BF), pltpu.VMEM((2, ny, ROWS, 128), BF),
         pltpu.VMEM((ROWS, 512), BF), pltpu.VMEM((ROWS, 512), BF),
-        dma((12,)), dma((6,)), dma((6,)), dma((6,)), dma((6,)), dma, dma,
+        dma((12,)), dma((6,)), dma((6,)), dma((6,)), dma((6,)), dma((6,)), dma((6,)), dma, dma,
         dma((nr,)), dma((nr,)), dma((nr,)), dma((nr,)), dma((nz,)), dma((nz,)), dma((nr,)), dma((nr,)),
         dma((far, 2)), dma((far, 2)), dma((far, 2)), dma((far, 2)),
         dma((nr,)), dma((nr,)), dma((2, ny)), dma((2, ny)),
     ]
-    mixed = pl.pallas_call(
+    return pl.pallas_call(
         functools.partial(kernel, nz, nx, ny),
-        out_shape=jax.ShapeDtypeStruct((ROWS, D), F32),
+        out_shape=jax.ShapeDtypeStruct((ROWS, D), BF),
         in_specs=[hbm if i in in_hbm else vmem for i in range(len(args))],
         out_specs=vmem,
         scratch_shapes=scratch,
@@ -634,7 +643,6 @@
         ),
         name="mixer",
     )(*args)
-    return mixed.astype(BF)
 
 
 def solution(mesh):

time: 56.3 us -> 54.6 us (0.970)
  other arithmetic: 1.77 us -> 0 us
  Pallas kernels: 54 us -> 52.3 us
  local copies, waits for them, and re-layouts: 0 us -> 1.67 us
    convert_element_type x1 -> x0, other arithmetic: 1.77 us -> none  [body(): return mixed.astype(BF)]
    pallas_call x1, Pallas kernels: 54 us -> 52.3 us  [body(): pl.pallas_call(functools.partial(kernel, nz, nx, ny), out_shape=jax.Shape...]
    unnamed x0 -> x1, local copies, waits for them, and re-layouts: none -> 1.67 us
where the time goes in v5:
time: 54.6 us; the launch traced here: 54 us
  Pallas kernels  52.3 us (96%)
  local copies, waits for them, and re-layouts  1.67 us (3%)
    pallas_call x1, Pallas kernels, body(): pl.pallas_call(functools.partial(kernel, nz, nx, ny), out_shape=jax.Shape...  52.3 us
    unnamed x1, local copies, waits for them, and re-layouts  1.67 us

profile of v5, /device:TPU:2, one launch (start us, length us, event | category | flops | bytes accessed | tf_op | source)
XLA Modules:
  0.0 54.0 jit_solution(2810399180890480463)
XLA Ops:
  0.0 52.3 %mixer.1 = bf16[64,2048]{1,0:T(8,128)(2,1)} custom-call(bf16[64,2048]{1,0:T(8,128)(2,1)} %tok.1, f32[1,2048]{1,0:T(1,128)} %bitcast.19, bf16[2048,128]{1,0:T(8,128)(2,1)} %hmq.1, bf16[2048,128]{1,0:T(8,128)(2,1)} %hmk.1, bf16[2048,128]{1,0:T(8,128)(2,1)} %hmv.1, bf16[2048,128]{1,0:T(8,128)(2,1)} %hmo.1, bf16[32,2048]{1,0:T(8,128)(2,1)} %bitcast.17, ...), custom_call_target="tpu_custom_call" | custom-call | tf_op jit(solution)/shard_map/mixer/pallas_call | solution.py:635
  52.3 1.7 %copy.22 = bf16[64,2048]{1,0:T(8,128)(2,1)} copy(bf16[64,2048]{1,0:T(8,128)(2,1)} %mixer.1) | data formatting | bytes 524288

commit v6 on v5

--- a/solution.py
+++ b/solution.py
@@ -59,13 +59,14 @@
 
 def kernel(
     nz, nx, ny,
-    tok, gain, hmq, hmk, hmv, hmo, hgt, goff, mng, hqd, qdg, hld, lg, hrt, hqt, hlup,
-    qgain, kgain, hwm, hwa,
+    htok, hgain, hmq, hmk, hmv, hmo, hgt, hgoff, hmng, hqd, hqdg, hld, hlg, hrt, hqt, hlup,
+    hqgain, hkgain, hwm, hwa,
     out,
+    tok, gain, goff, mng, qdg, lg, qgain, kgain,
     mq, mk, mv, mo, gt, qd, ld, rt, qt, lup, wm, wa,
     rt4, wqt, lupf, trig, normed, ebuf, qbuf, kvg, psend, qsend, qg, asend, agot, rtot, pb, csend, cgot,
     memp, memg, qop, kop, vt, acc_s, top_s, osend, po, fsend, fx, lhs_m, lhs_a,
-    w_sem, n_ss, n_rs, e_ss, e_rs, l_ss, l_rs, p_ss, p_rs, q_ss, q_rs, a_ss, a_rs, b_ss, b_rs, c_ss, c_rs,
+    w_sem, s_sem, n_ss, n_rs, e_ss, e_rs, l_ss, l_rs, p_ss, p_rs, q_ss, q_rs, a_ss, a_rs, b_ss, b_rs, c_ss, c_rs,
     u_ss, u_rs, d_ss, d_rs, o_ss, o_rs, f_ss, f_rs,
 ):
     z = lax.axis_index("sp_0")
@@ -87,17 +88,16 @@
 
     pairs = ((hld, ld), (hrt, rt), (hqd, qd), (hlup, lup), (hqt, qt), (hmq, mq), (hmk, mk), (hmv, mv),
              (hgt, gt), (hmo, mo), (hwm, wm), (hwa, wa))
+    smalls = ((htok, tok), (hgain, gain), (hqgain, qgain), (hkgain, kgain), (hlg, lg), (hqdg, qdg), (hgoff, goff),
+              (hmng, mng))
+    first_loads = [pltpu.make_async_copy(a, b, s_sem.at[i]) for i, (a, b) in enumerate(smalls)]
     loads = [pltpu.make_async_copy(a, b, w_sem.at[i]) for i, (a, b) in enumerate(pairs)]
-    for load in loads:
+    for load in first_loads + loads[:2]:
         load.start()
     barrier = pltpu.get_barrier_semaphore()
     peers = [at_y(d) for d in range(1, ny)] + [at_row(d) for d in range(1, nr)] + [at_z(d) for d in range(1, nz)]
     for peer in peers:
         pl.semaphore_signal(barrier, inc=1, device_id=peer, device_id_type=MESH)
-
-    xt = tok[...].astype(F32)
-    normed_local = (rms(xt) * gain[...]).astype(BF)
-    normed[pl.ds(y, 1)] = normed_local[None]
 
     segment = (z * nx + x) * 2 + c
     places = (segment * BLOCK + lax.broadcasted_iota(jnp.int32, (16, BLOCK), 1)).astype(F32)
@@ -108,6 +108,14 @@
     angles = places * frequency
     trig[0] = jnp.transpose(jnp.concatenate([jnp.cos(angles)] * 8, axis=0))
     trig[1] = jnp.transpose(jnp.concatenate([jnp.sin(angles)] * 8, axis=0))
+
+    for load in first_loads:
+        load.wait()
+    for load in loads[2:]:
+        load.start()
+    xt = tok[...].astype(F32)
+    normed_local = (rms(xt) * gain[...]).astype(BF)
+    normed[pl.ds(y, 1)] = normed_local[None]
 
     src = lax.broadcasted_iota(jnp.int32, (96, 128), 0)
     dst = lax.broadcasted_iota(jnp.int32, (96, 128), 1)
@@ -165,7 +173,7 @@
     for copy in l_direct:
         copy.start()
     loads[3].wait()
-    lupf[...] = lup[...].astype(F32)
+    lupf[pl.ds(0, 8 * KVR), :] = lup[...].astype(F32)
     loads[4].wait()
     for h in range(2):
         base = 96 * (2 * y + h)
@@ -604,17 +612,18 @@
         memory_output, attention_output,
     )
     nr = nx * 2
-    in_hbm = {2, 3, 4, 5, 6, 9, 11, 13, 14, 15, 18, 19}
     vmem = pl.BlockSpec(memory_space=pltpu.VMEM)
     hbm = pl.BlockSpec(memory_space=pltpu.HBM)
     dma = pltpu.SemaphoreType.DMA
     keys = nz * 512
     far = nz // 2 + 1
     scratch = [
+        pltpu.VMEM((ROWS, D), BF), pltpu.VMEM((1, D), F32), pltpu.VMEM((4, 2, BLOCK), F32), pltpu.VMEM((4, 128), F32),
+        pltpu.VMEM((3, 128), F32), pltpu.VMEM((1, KVR), F32), pltpu.VMEM((1, 96), F32), pltpu.VMEM((1, 96), F32),
         pltpu.VMEM((D, 128), BF), pltpu.VMEM((D, 128), BF), pltpu.VMEM((D, 128), BF), pltpu.VMEM((D, 128), BF),
         pltpu.VMEM((32, D), BF), pltpu.VMEM((D, QR), BF), pltpu.VMEM((D, KVR), BF), pltpu.VMEM((32, D), BF),
         pltpu.VMEM((768, QR), BF), pltpu.VMEM((KVR * 8, 128), BF), pltpu.VMEM((512, D), BF), pltpu.VMEM((512, D), BF),
-        pltpu.VMEM((256, D), BF), pltpu.VMEM((2, 128, QR), BF), pltpu.VMEM((KVR * 8, 128), F32),
+        pltpu.VMEM((256, D), BF), pltpu.VMEM((2, 128, QR), BF), pltpu.VMEM((KVR * 8 + 8, 128), F32),
         pltpu.VMEM((2, BLOCK, 128), F32),
         pltpu.VMEM((ny, ROWS, D), BF), pltpu.VMEM((ny, ROWS, 384), BF), pltpu.VMEM((ny, ROWS, QR), BF),
         pltpu.VMEM((nz, 2, BLOCK + ROWS, 128), BF), pltpu.VMEM((BLOCK + ROWS, 128), BF),
@@ -627,7 +636,7 @@
         pltpu.VMEM((nr, 144, 128), BF), pltpu.VMEM((nr, 144, 128), BF),
         pltpu.VMEM((2, ny, ROWS, 128), BF), pltpu.VMEM((2, ny, ROWS, 128), BF),
         pltpu.VMEM((ROWS, 512), BF), pltpu.VMEM((ROWS, 512), BF),
-        dma((12,)), dma((6,)), dma((6,)), dma((6,)), dma((6,)), dma((6,)), dma((6,)), dma, dma,
+        dma((12,)), dma((8,)), dma((6,)), dma((6,)), dma((6,)), dma((6,)), dma((6,)), dma((6,)), dma, dma,
         dma((nr,)), dma((nr,)), dma((nr,)), dma((nr,)), dma((nz,)), dma((nz,)), dma((nr,)), dma((nr,)),
         dma((far, 2)), dma((far, 2)), dma((far, 2)), dma((far, 2)),
         dma((nr,)), dma((nr,)), dma((2, ny)), dma((2, ny)),
@@ -635,7 +644,7 @@
     return pl.pallas_call(
         functools.partial(kernel, nz, nx, ny),
         out_shape=jax.ShapeDtypeStruct((ROWS, D), BF),
-        in_specs=[hbm if i in in_hbm else vmem for i in range(len(args))],
+        in_specs=[hbm] * len(args),
         out_specs=vmem,
         scratch_shapes=scratch,
         compiler_params=pltpu.CompilerParams(

time: 54.6 us -> 54 us (0.989)
  Pallas kernels: 52.3 us -> 51.7 us
    pallas_call x1, Pallas kernels: 52.3 us -> 51.7 us  [body(): pl.pallas_call(functools.partial(kernel, nz, nx, ny), out_shape=jax.Shape...]
where the time goes in v6:
time: 54 us; the launch traced here: 53.4 us
  Pallas kernels  51.7 us (96%)
  local copies, waits for them, and re-layouts  1.67 us (3%)
    pallas_call x1, Pallas kernels, body(): pl.pallas_call(functools.partial(kernel, nz, nx, ny), out_shape=jax.Shape...  51.7 us
    unnamed x1, local copies, waits for them, and re-layouts  1.67 us

profile of v6, /device:TPU:2, one launch (start us, length us, event | category | flops | bytes accessed | tf_op | source)
XLA Modules:
  0.0 53.4 jit_solution(15378094872584880889)
XLA Ops:
  0.0 51.7 %mixer.1 = bf16[64,2048]{1,0:T(8,128)(2,1)} custom-call(bf16[64,2048]{1,0:T(8,128)(2,1)} %htok.1, f32[1,2048]{1,0:T(1,128)} %bitcast.19, bf16[2048,128]{1,0:T(8,128)(2,1)} %hmq.1, bf16[2048,128]{1,0:T(8,128)(2,1)} %hmk.1, bf16[2048,128]{1,0:T(8,128)(2,1)} %hmv.1, bf16[2048,128]{1,0:T(8,128)(2,1)} %hmo.1, bf16[32,2048]{1,0:T(8,128)(2,1)} %bitcast.17, ...), custom_call_target="tpu_custom_call" | custom-call | tf_op jit(solution)/shard_map/mixer/pallas_call | solution.py:644
  51.7 1.7 %copy.22 = bf16[64,2048]{1,0:T(8,128)(2,1)} copy(bf16[64,2048]{1,0:T(8,128)(2,1)} %mixer.1) | data formatting | bytes 524288

commit v7 on v6

--- a/solution.py
+++ b/solution.py
@@ -296,6 +296,8 @@
     def attend(begin, end, slots, start=False, last=False):
         def block(n, carry):
             i = lax.rem(n + nx - 1, nx) if start else n
+            if last:
+                i = jnp.where(n < 2, 1 - n, n)
             xx = lax.rem(x + i + 1, nx)
             cores = [lax.rem(c + t, 2) for t in range(2)]
             qv = jnp.concatenate([qop[2 * xx + cores[t]] for t in range(2)], axis=0)
@@ -343,23 +345,29 @@
         loads[i].wait()
     loads[9].wait()
 
+    def project_gate(slot):
+        at = pl.ds(pl.multiple_of(slot * ROWS, ROWS), ROWS)
+        memp[3, at, :] = dot(normed[slot], mo[...]).astype(BF)
+
     def project(slot):
         part = normed[slot]
         at = pl.ds(pl.multiple_of(slot * ROWS, ROWS), ROWS)
         memp[0, at, :] = dot(part, mq[...]).astype(BF)
         memp[1, at, :] = (dot(part, mk[...]) * 0.125).astype(BF)
         memp[2, at, :] = dot(part, mv[...]).astype(BF)
-        memp[3, at, :] = dot(part, mo[...]).astype(BF)
         memg[at, :] = dot_nt(part, gt[...]).astype(BF)
 
     for i in range(2):
         n_direct[i].wait_recv()
         n_onward[i].start()
     project(y)
+    project_gate(y)
     n_direct[2].wait_recv()
     n_direct[3].wait_recv()
     project(lax.rem(y + 1, ny))
     project(lax.rem(y + ny - 1, ny))
+    project_gate(lax.rem(y + 1, ny))
+    project_gate(lax.rem(y + ny - 1, ny))
     ring_recv(1, 0)
     take_queries(nx - 1)
     ring_recv(1, 1)
@@ -510,6 +518,7 @@
         own_parts.append((
             jnp.where(low, nums[0], nums[1]), jnp.where(low, dens[0], dens[1]), jnp.where(low, tops[0], tops[1]), cum
         ))
+    project_gate(lax.rem(y + 2, ny))
     out_gate = jax.nn.sigmoid(memp[3].astype(F32))
     for copy in c_copies:
         copy.wait_recv()

time: 54 us -> 53.8 us (level)
  no operation moved by 1% of the time
where the time goes in v7:
time: 53.8 us; the launch traced here: 53.3 us
  Pallas kernels  51.6 us (96%)
  local copies, waits for them, and re-layouts  1.67 us (3%)
    pallas_call x1, Pallas kernels, body(): pl.pallas_call(functools.partial(kernel, nz, nx, ny), out_shape=jax.Shape...  51.6 us
    unnamed x1, local copies, waits for them, and re-layouts  1.67 us

profile of v7, /device:TPU:2, one launch (start us, length us, event | category | flops | bytes accessed | tf_op | source)
XLA Modules:
  0.0 53.3 jit_solution(15067288446237417917)
XLA Ops:
  0.0 51.6 %mixer.1 = bf16[64,2048]{1,0:T(8,128)(2,1)} custom-call(bf16[64,2048]{1,0:T(8,128)(2,1)} %htok.1, f32[1,2048]{1,0:T(1,128)} %bitcast.19, bf16[2048,128]{1,0:T(8,128)(2,1)} %hmq.1, bf16[2048,128]{1,0:T(8,128)(2,1)} %hmk.1, bf16[2048,128]{1,0:T(8,128)(2,1)} %hmv.1, bf16[2048,128]{1,0:T(8,128)(2,1)} %hmo.1, bf16[32,2048]{1,0:T(8,128)(2,1)} %bitcast.17, ...), custom_call_target="tpu_custom_call" | custom-call | tf_op jit(solution)/shard_map/mixer/pallas_call | solution.py:653
  51.6 1.7 %copy.22 = bf16[64,2048]{1,0:T(8,128)(2,1)} copy(bf16[64,2048]{1,0:T(8,128)(2,1)} %mixer.1) | data formatting | bytes 524288
